TPU v7x, 512 devices: a 4x2x32 block of a 4x8x32 slice. The times are simulated.
512 devices in a mesh: grp: 2 (over y), sp: 32 (over z), tp: 8 (over x, core).
Axes of the slice: x: 4, y: 2, z: 32, core: 2. Of those that a mesh axis runs over, the one named last changes fastest.
The devices are a block of a 4x8x32 slice.
Arguments:
- tokens: bfloat16 [24576, 2048], P(('grp', 'sp')), parts along dimension 0, may hold values from -6 to 6
- norm_gain: float32 [2048], replicated, may hold values from 0.1 to 1.9
- w_query: bfloat16 [2048, 1024], P(None, 'tp'), may hold values from -0.088388348 to 0.088388348
- w_key: bfloat16 [2048, 1024], P(None, 'tp'), may hold values from -1.5467961 to 1.5467961
- w_value: bfloat16 [2048, 1024], P(None, 'tp'), may hold values from -0.30935922 to 0.30935922
- out_gain: float32 [1024], P('tp'), may hold values from 0.1 to 1.9
- w_out: bfloat16 [1024, 2048], P('tp'), may hold values from -0.1875 to 0.1875
Outputs:
- mixed: bfloat16 [24576, 2048], P(('grp', 'sp', 'tp')), parts along dimension 0
There are 2 independent parts, one for each index of `grp`. A program takes and returns all parts, laid end to end along the dimension named above; an argument that names none is the same for every part. Nothing has to cross between parts.
All inputs are finite; a program needn't handle non-finite values.
Results may differ from a plain program's by a relative error of at most 0.015.
Values may be sent and summed in bfloat16 or wider, within the bound.
No kernel may reach another device: no remote copies, remote signals or barrier semaphores. Data moves between devices by JAX's collectives and lax.ppermute only.
A program may use at most 64 MiB of HBM per device.

v0:
```python
from functools import reduce

import jax
import jax.numpy as jnp
from jax import lax
from jax.sharding import PartitionSpec as P

HEAD_DIM = 64
WINDOW_FIRST = 128
WINDOW_SECOND = 512
DILATION_SECOND = 4
WINDOW_THIRD = 2048
DILATION_THIRD = 16


EPS = 1e-06
NEG = -1e30


def from_behind(value, axis, steps):
    count = lax.axis_size(axis)
    initial, last = (max(0, -steps), min(count, count - steps))
    return lax.ppermute(value, axis, [(source, source + steps) for source in range(initial, last)])


def copy_for_each(value, axis):
    copies = jnp.broadcast_to(value, (lax.axis_size(axis), *value.shape))
    return lax.all_to_all(copies, axis, split_axis=0, concat_axis=0, tiled=True)


def taken_together(value, axis):
    everything = copy_for_each(value, axis)
    return jnp.sum(everything, axis=0)


def in_blocks(value, dim, count):
    before, after = (value.shape[:dim], value.shape[dim + 1 :])
    return jnp.moveaxis(value.reshape(*before, count, -1, *after), dim, 0)


def sum_at_owner(value, axis, dim):
    tiles = in_blocks(value, dim, lax.axis_size(axis))
    arrived = lax.all_to_all(tiles, axis, split_axis=0, concat_axis=0, tiled=True)
    return arrived.astype(jnp.float32).sum(axis=0)


def band_part(queries, key_rows, value_rows, span_len, dilation_step, first_key):
    query_len, head_count, head_width = queries.shape
    class_len = query_len // dilation_step
    block_len = class_len if class_len <= 128 else 128
    blocks = class_len // block_len
    window_len = block_len + span_len
    query_blk = queries.reshape(blocks, block_len, dilation_step, head_count, head_width)
    key_cls = key_rows.reshape(class_len + span_len, dilation_step, head_count, head_width)
    value_cls = value_rows.reshape(class_len + span_len, dilation_step, head_count, head_width)
    key_blk = jnp.stack(
        [
            key_cls[block_idx * block_len : block_idx * block_len + window_len]
            for block_idx in range(blocks)
        ]
    )
    value_blk = jnp.stack(
        [
            value_cls[block_idx * block_len : block_idx * block_len + window_len]
            for block_idx in range(blocks)
        ]
    )
    scores = jnp.einsum(
        "jqchx,jkchx->jchqk", query_blk, key_blk, preferred_element_type=jnp.float32
    ) * HEAD_DIM ** (-0.5)
    lag_steps = (
        span_len
        + jnp.arange(block_len, dtype=jnp.int32)[:, None]
        - jnp.arange(window_len, dtype=jnp.int32)[None, :]
    )
    inside = (lag_steps >= 0) & (lag_steps <= span_len)
    key_pos = (
        first_key
        + (
            jnp.arange(blocks, dtype=jnp.int32)[:, None, None] * block_len
            + jnp.arange(window_len, dtype=jnp.int32)[None, None, :]
        )
        * dilation_step
        + jnp.arange(dilation_step, dtype=jnp.int32)[None, :, None]
    )
    usable = inside[None, None, None] & (key_pos >= 0)[:, :, None, None, :]
    scores = jnp.where(usable, scores, NEG)
    row_max = jnp.max(scores, axis=-1)
    weights = jnp.exp(scores - row_max[..., None])
    row_sum = jnp.sum(weights, axis=-1)
    weighted = jnp.einsum(
        "jchqk,jkchx->jqchx",
        weights.astype(jnp.bfloat16),
        value_blk,
        preferred_element_type=jnp.float32,
    )
    weighted = weighted.reshape(query_len, head_count, head_width)
    row_max = jnp.transpose(row_max, (0, 3, 1, 2)).reshape(query_len, head_count)
    row_sum = jnp.transpose(row_sum, (0, 3, 1, 2)).reshape(query_len, head_count)
    return (weighted, row_max, row_sum)


def mixture(pattern_out):
    peak_max = reduce(jnp.maximum, [result[1] for result in pattern_out])
    numerator = reduce(
        lambda left, right: left + right,
        [jnp.exp(result[1] - peak_max)[..., None] * result[0] for result in pattern_out],
    )
    denominator = reduce(
        lambda left, right: left + right,
        [jnp.exp(result[1] - peak_max) * result[2] for result in pattern_out],
    )
    return numerator / denominator[..., None]


def on_device(tokens, norm_gain, w_query, w_key, w_value, out_gain, w_out):
    tok_rows = tokens.shape[0]
    inverse = lax.rsqrt(jnp.mean(jnp.square(tokens.astype(jnp.float32)), axis=-1) + EPS)
    scaled = (tokens * norm_gain).astype(jnp.bfloat16)

    def project(weight):
        return (
            jnp.dot(scaled, weight, preferred_element_type=jnp.float32) * inverse[:, None]
        ).astype(jnp.bfloat16)

    queries = project(w_query)
    key_rows = project(w_key)
    value_rows = project(w_value)
    channels = w_query.shape[1]
    head_count = channels // HEAD_DIM
    offset = lax.axis_index("sp") * tok_rows
    reach_devs = min(-(-WINDOW_THIRD // tok_rows), lax.axis_size("sp") - 1)
    key_value = (key_rows, value_rows)
    older_keys = []
    older_values = []
    current = key_value
    for distance in range(reach_devs):
        current = from_behind((current[0], current[1]), "sp", 1)
        older_keys.insert(0, current[0])
        older_values.insert(0, current[1])
    excess = reach_devs * tok_rows - WINDOW_THIRD
    far_keys = jnp.concatenate(older_keys, axis=0)[excess:]
    far_values = jnp.concatenate(older_values, axis=0)[excess:]
    query_heads = queries.reshape(tok_rows, head_count, HEAD_DIM)
    pattern_out = []
    for window_span, dilation_step in (
        (WINDOW_FIRST, 1),
        (WINDOW_SECOND, DILATION_SECOND),
        (WINDOW_THIRD, DILATION_THIRD),
    ):
        keys_ext = jnp.concatenate(
            [far_keys[WINDOW_THIRD - window_span :], key_rows], axis=0
        ).reshape(window_span + tok_rows, head_count, HEAD_DIM)
        values_ext = jnp.concatenate(
            [far_values[WINDOW_THIRD - window_span :], value_rows], axis=0
        ).reshape(window_span + tok_rows, head_count, HEAD_DIM)
        pattern_out.append(
            band_part(
                query_heads,
                keys_ext,
                values_ext,
                window_span // dilation_step,
                dilation_step,
                offset - window_span,
            )
        )
    attended = mixture(pattern_out).reshape(tok_rows, channels)
    squares = taken_together(jnp.sum(attended * attended, axis=-1), "tp")
    out_scale = lax.rsqrt(squares / (channels * lax.axis_size("tp")) + EPS)
    gated = (attended * out_gain).astype(jnp.bfloat16)
    share_rows = tok_rows // lax.axis_size("tp")
    summed = sum_at_owner(
        jnp.dot(gated, w_out, preferred_element_type=jnp.float32).astype(jnp.bfloat16), "tp", 0
    )
    own_scale = lax.dynamic_slice_in_dim(
        out_scale, lax.axis_index("tp") * share_rows, share_rows, 0
    )
    return (summed * own_scale[:, None]).astype(jnp.bfloat16)


def solution(mesh):
    in_specs = (
        P(("grp", "sp"), None),
        P(),
        P(None, "tp"),
        P(None, "tp"),
        P(None, "tp"),
        P("tp"),
        P("tp", None),
    )
    out_specs = P(("grp", "sp", "tp"), None)
    return jax.shard_map(
        on_device, mesh=mesh, in_specs=in_specs, out_specs=out_specs, check_vma=False
    )
```

profile of v0, /device:TPU:33, one launch (start us, length us, event | category | flops | bytes accessed | tf_op | source)
XLA Modules:
  0.0 142.6 jit_solution(3823618872502265341)
XLA Ops:
  0.0 1.9 %fusion.1 = f32[384]{0:T(512)S(1)} fusion(bf16[384,2048]{1,0:T(8,128)(2,1)} %param.7), kind=kLoop, calls=%fused_computation.3 | loop fusion | flops 2358912 | bytes 1574400 | tf_op jit(solution)/shard_map/reduce_sum | solution.py:118
  2.0 1.7 %fusion.26 = bf16[384,128]{1,0:T(8,128)(2,1)S(1)} fusion(bf16[2048,128]{1,0:T(8,128)(2,1)} %param.11, bf16[384,2048]{1,0:T(8,128)(2,1)S(1)} %copy-done.1, f32[2048]{0:T(1024)} %param.8, f32[384]{0:T(512)S(1)} %add_rsqrt_fusion.1), kind=kOutput, calls=%fused_computation.24 | convolution fusion | flops 203784192 | bytes 2205184 | tf_op jit(solution)/shard_map/dot_general | solution.py:123
  3.7 5.4 %collective-permute-start.6 = (bf16[384,128]{1,0:T(8,128)(2,1)S(1)}, bf16[384,128]{1,0:T(8,128)(2,1)S(1)}, u32[]{:S(2)}, u32[]{:S(2)}) collective-permute-start(bf16[384,128]{1,0:T(8,128)(2,1)S(1)} %fusion.26), channel_id=1, source_target_pairs={{0,8},{8,16},{16,24},{24,32},{32,40},{40,48},{48,56},{56,64},{64,7... | collective-permute-start | bytes 294920 | tf_op jit(solution)/shard_map/ppermute | solution.py:23
  9.7 4.4 %collective-permute-start = (bf16[384,128]{1,0:T(8,128)(2,1)S(1)}, bf16[384,128]{1,0:T(8,128)(2,1)S(1)}, u32[]{:S(2)}, u32[]{:S(2)}) collective-permute-start(bf16[384,128]{1,0:T(8,128)(2,1)S(1)} %fusion.29), channel_id=1, source_target_pairs={{0,8},{8,16},{16,24},{24,32},{32,40},{40,48},{48,56},{56,64},{64,7... | collective-permute-start | bytes 294920 | tf_op jit(solution)/shard_map/ppermute | solution.py:23
  20.1 4.4 %collective-permute-start.7 = (bf16[384,128]{1,0:T(8,128)(2,1)S(1)}, bf16[384,128]{1,0:T(8,128)(2,1)S(1)}, u32[]{:S(2)}, u32[]{:S(2)}) collective-permute-start(bf16[384,128]{1,0:T(8,128)(2,1)S(1)} %collective-permute-done.6), channel_id=1, source_target_pairs={{0,8},{8,16},{16,24},{24,32},{32,40},{40,48},{48,56},{56,64},{64,7... | collective-permute-start | bytes 294920 | tf_op jit(solution)/shard_map/ppermute | solution.py:23
  24.6 5.6 %collective-permute-start.1 = (bf16[384,128]{1,0:T(8,128)(2,1)S(1)}, bf16[384,128]{1,0:T(8,128)(2,1)S(1)}, u32[]{:S(2)}, u32[]{:S(2)}) collective-permute-start(bf16[384,128]{1,0:T(8,128)(2,1)S(1)} %collective-permute-done), channel_id=1, source_target_pairs={{0,8},{8,16},{16,24},{24,32},{32,40},{40,48},{48,56},{56,64},{64,7... | collective-permute-start | bytes 294920 | tf_op jit(solution)/shard_map/ppermute | solution.py:23
  30.5 1.3 collective-permute-done.1
  32.1 4.4 %collective-permute-start.8 = (bf16[384,128]{1,0:T(8,128)(2,1)S(1)}, bf16[384,128]{1,0:T(8,128)(2,1)S(1)}, u32[]{:S(2)}, u32[]{:S(2)}) collective-permute-start(bf16[384,128]{1,0:T(8,128)(2,1)S(1)} %collective-permute-done.7), channel_id=1, source_target_pairs={{0,8},{8,16},{16,24},{24,32},{32,40},{40,48},{48,56},{56,64},{64,7... | collective-permute-start | bytes 294920 | tf_op jit(solution)/shard_map/ppermute | solution.py:23
  36.5 1.4 fusion.89
  37.9 5.1 %collective-permute-start.2 = (bf16[384,128]{1,0:T(8,128)(2,1)S(1)}, bf16[384,128]{1,0:T(8,128)(2,1)}, u32[]{:S(2)}, u32[]{:S(2)}) collective-permute-start(bf16[384,128]{1,0:T(8,128)(2,1)S(1)} %collective-permute-done.1), channel_id=1, source_target_pairs={{0,8},{8,16},{16,24},{24,32},{32,40},{40,48},{48,56},{56,64},{64,7... | collective-permute-start | bytes 294920 | tf_op jit(solution)/shard_map/ppermute | solution.py:23
  43.0 4.5 %collective-permute-start.9 = (bf16[384,128]{1,0:T(8,128)(2,1)S(1)}, bf16[384,128]{1,0:T(8,128)(2,1)}, u32[]{:S(2)}, u32[]{:S(2)}) collective-permute-start(bf16[384,128]{1,0:T(8,128)(2,1)S(1)} %collective-permute-done.8), channel_id=1, source_target_pairs={{0,8},{8,16},{16,24},{24,32},{32,40},{40,48},{48,56},{56,64},{64,7... | collective-permute-start | bytes 294920 | tf_op jit(solution)/shard_map/ppermute | solution.py:23
  47.7 5.7 %collective-permute-start.3 = (bf16[384,128]{1,0:T(8,128)(2,1)}, bf16[384,128]{1,0:T(8,128)(2,1)}, u32[]{:S(2)}, u32[]{:S(2)}) collective-permute-start(bf16[384,128]{1,0:T(8,128)(2,1)} %collective-permute-done.2), channel_id=1, source_target_pairs={{0,8},{8,16},{16,24},{24,32},{32,40},{40,48},{48,56},{56,64},{64,7... | collective-permute-start | bytes 294920 | tf_op jit(solution)/shard_map/ppermute | solution.py:23
  53.4 4.5 %collective-permute-start.10 = (bf16[384,128]{1,0:T(8,128)(2,1)}, bf16[384,128]{1,0:T(8,128)(2,1)}, u32[]{:S(2)}, u32[]{:S(2)}) collective-permute-start(bf16[384,128]{1,0:T(8,128)(2,1)} %collective-permute-done.9), channel_id=1, source_target_pairs={{0,8},{8,16},{16,24},{24,32},{32,40},{40,48},{48,56},{56,64},{64,7... | collective-permute-start | bytes 294920 | tf_op jit(solution)/shard_map/ppermute | solution.py:23
  58.8 4.5 %collective-permute-start.4 = (bf16[384,128]{1,0:T(8,128)(2,1)}, bf16[384,128]{1,0:T(8,128)(2,1)}, u32[]{:S(2)}, u32[]{:S(2)}) collective-permute-start(bf16[384,128]{1,0:T(8,128)(2,1)} %collective-permute-done.3), channel_id=1, source_target_pairs={{0,8},{8,16},{16,24},{24,32},{32,40},{40,48},{48,56},{56,64},{64,7... | collective-permute-start | bytes 294920 | tf_op jit(solution)/shard_map/ppermute | solution.py:23
  63.3 4.4 %collective-permute-start.11 = (bf16[384,128]{1,0:T(8,128)(2,1)}, bf16[384,128]{1,0:T(8,128)(2,1)}, u32[]{:S(2)}, u32[]{:S(2)}) collective-permute-start(bf16[384,128]{1,0:T(8,128)(2,1)} %collective-permute-done.10), channel_id=1, source_target_pairs={{0,8},{8,16},{16,24},{24,32},{32,40},{40,48},{48,56},{56,64},{64,7... | collective-permute-start | bytes 294920 | tf_op jit(solution)/shard_map/ppermute | solution.py:23
  70.3 0.8 copy.214
  71.1 0.8 copy.226
  71.9 5.7 %collective-permute-start.5 = (bf16[384,128]{1,0:T(8,128)(2,1)}, bf16[384,128]{1,0:T(8,128)(2,1)}, u32[]{:S(2)}, u32[]{:S(2)}) collective-permute-start(bf16[384,128]{1,0:T(8,128)(2,1)} %collective-permute-done.4), channel_id=1, source_target_pairs={{0,8},{8,16},{16,24},{24,32},{32,40},{40,48},{48,56},{56,64},{64,7... | collective-permute-start | bytes 294920 | tf_op jit(solution)/shard_map/ppermute | solution.py:23
  77.5 0.9 constant_dynamic-update-slice_fusion.11
  78.4 0.9 constant_dynamic-update-slice_fusion.10
  79.4 0.9 constant_dynamic-update-slice_fusion.9
  81.0 0.9 constant_dynamic-update-slice_fusion.5
  81.9 0.9 constant_dynamic-update-slice_fusion.4
  82.8 0.9 constant_dynamic-update-slice_fusion.3
  83.7 0.9 constant_dynamic-update-slice_fusion.2
  84.8 1.6 %reshape.488 = bf16[152,16,2,64]{3,2,1,0:T(2,128)(2,1)} reshape(bf16[2432,128]{1,0:T(8,128)(2,1)S(1)} %pad_maximum_fusion) | data formatting | bytes 1245184 | tf_op jit(solution)/shard_map/reshape.39
  86.3 2.2 %fusion.88 = (f32[16,2,24]{2,1,0:T(2,128)S(1)}, f32[16,2,24,152]{3,2,1,0:T(8,128)S(1)}) fusion(bf16[152,16,2,64]{3,2,1,0:T(2,128)(2,1)} %reshape.488, bf16[24,16,2,64]{3,2,1,0:T(2,128)(2,1)S(1)} %copy-done.9, pred[16,24,152]{2,1,0:T(8,128)(4,1)S(1)} %copy-done.13), kind=kOutput, calls=%fused_computation.132 | convolution fusion | flops 15291648 | bytes 1249280 | tf_op jit(solution)/shard_map/jqchx,jkchx->jchqk/dot_general | solution.py:68
  92.2 19.9 %all-to-all-start.1 = ((f32[8,1,384]{2,1,0:T(1,128)}), f32[8,1,384]{2,1,0:T(1,128)S(1)}, u32[]{:S(2)}, u32[]{:S(2)}) async-start(f32[8,1,384]{2,1,0:T(1,128)} %broadcast_in_dim.40), calls=%async_computation.1 | async-start | bytes 24576 | tf_op jit(solution)/shard_map/all_to_all | solution.py:28
  112.2 1.8 %convolution_convert_fusion = bf16[384,2048]{1,0:T(8,128)(2,1)} fusion(bf16[384,128]{0,1:T(8,128)(2,1)S(1)} %fusion.66, bf16[128,2048]{1,0:T(8,128)(2,1)S(1)} %copy-done), kind=kOutput, calls=%fused_computation.5 | convolution fusion | flops 202113024 | bytes 2195456 | tf_op jit(solution)/shard_map/dot_general | solution.py:173
  114.0 2.8 %all-to-all-done.1 = f32[8,1,384]{2,1,0:T(1,128)S(1)} async-done(((f32[8,1,384]{2,1,0:T(1,128)}), f32[8,1,384]{2,1,0:T(1,128)S(1)}, u32[]{:S(2)}, u32[]{:S(2)}) %all-to-all-start.1) | async-done | bytes 12320 | tf_op jit(solution)/shard_map/all_to_all | solution.py:28
  116.7 4.2 %all-to-all-start = ((bf16[8,48,2048]{2,1,0:T(8,128)(2,1)}), bf16[8,48,2048]{2,1,0:T(8,128)(2,1)S(1)}, u32[]{:S(2)}, u32[]{:S(2)}) async-start(bf16[8,48,2048]{2,1,0:T(8,128)(2,1)} %bitcast.40), calls=%async_computation | async-start | bytes 3145728 | tf_op jit(solution)/shard_map/all_to_all | solution.py:43
  121.0 20.6 %all-to-all-done = bf16[8,48,2048]{2,1,0:T(8,128)(2,1)S(1)} async-done(((bf16[8,48,2048]{2,1,0:T(8,128)(2,1)}), bf16[8,48,2048]{2,1,0:T(8,128)(2,1)S(1)}, u32[]{:S(2)}, u32[]{:S(2)}) %all-to-all-start) | async-done | bytes 1572896 | tf_op jit(solution)/shard_map/all_to_all | solution.py:43
  (137 shorter events, 16.1 us)
Async XLA Ops:
  0.0 112.2 %copy-start = (bf16[128,2048]{1,0:T(8,128)(2,1)S(1)}, bf16[128,2048]{1,0:T(8,128)(2,1)}, u32[]{:S(2)}) copy-start(bf16[128,2048]{1,0:T(8,128)(2,1)} %param.13) | copy-start | bytes 1572868
  0.0 2.0 %copy-start.1 = (bf16[384,2048]{1,0:T(8,128)(2,1)S(1)}, bf16[384,2048]{1,0:T(8,128)(2,1)}, u32[]{:S(2)}) copy-start(bf16[384,2048]{1,0:T(8,128)(2,1)} %param.7) | copy-start | bytes 4718596
  1.9 7.1 %copy-start.19 = (bf16[2048,128]{1,0:T(8,128)(2,1)S(1)}, bf16[2048,128]{1,0:T(8,128)(2,1)}, u32[]{:S(2)}) copy-start(bf16[2048,128]{1,0:T(8,128)(2,1)} %param.10) | copy-start | bytes 1572868
  2.0 7.2 %copy-start.21 = (f32[2048]{0:T(1024)S(1)}, f32[2048]{0:T(1024)}, u32[]{:S(2)}) copy-start(f32[2048]{0:T(1024)} %param.8) | copy-start | bytes 24580
  3.7 10.5 %copy-start.20 = (bf16[2048,128]{1,0:T(8,128)(2,1)S(1)}, bf16[2048,128]{1,0:T(8,128)(2,1)}, u32[]{:S(2)}) copy-start(bf16[2048,128]{1,0:T(8,128)(2,1)} %param.9) | copy-start | bytes 1572868
  3.7 14.4 %collective-permute-start.6 = (bf16[384,128]{1,0:T(8,128)(2,1)S(1)}, bf16[384,128]{1,0:T(8,128)(2,1)S(1)}, u32[]{:S(2)}, u32[]{:S(2)}) collective-permute-start(bf16[384,128]{1,0:T(8,128)(2,1)S(1)} %fusion.26), channel_id=1, source_target_pairs={{0,8},{8,16},{16,24},{24,32},{32,40},{40,48},{48,56},{56,64},{64,7... | collective-permute-start | bytes 294920 | tf_op jit(solution)/shard_map/ppermute | solution.py:23
  9.7 8.0 %collective-permute-start = (bf16[384,128]{1,0:T(8,128)(2,1)S(1)}, bf16[384,128]{1,0:T(8,128)(2,1)S(1)}, u32[]{:S(2)}, u32[]{:S(2)}) collective-permute-start(bf16[384,128]{1,0:T(8,128)(2,1)S(1)} %fusion.29), channel_id=1, source_target_pairs={{0,8},{8,16},{16,24},{24,32},{32,40},{40,48},{48,56},{56,64},{64,7... | collective-permute-start | bytes 294920 | tf_op jit(solution)/shard_map/ppermute | solution.py:23
  18.1 29.4 %copy-start.3 = (bf16[384,128]{1,0:T(8,128)(2,1)}, bf16[384,128]{1,0:T(8,128)(2,1)S(1)}, u32[]{:S(2)}) copy-start(bf16[384,128]{1,0:T(8,128)(2,1)S(1)} %collective-permute-done.6) | copy-start | bytes 294916
  20.1 12.0 %collective-permute-start.7 = (bf16[384,128]{1,0:T(8,128)(2,1)S(1)}, bf16[384,128]{1,0:T(8,128)(2,1)S(1)}, u32[]{:S(2)}, u32[]{:S(2)}) collective-permute-start(bf16[384,128]{1,0:T(8,128)(2,1)S(1)} %collective-permute-done.6), channel_id=1, source_target_pairs={{0,8},{8,16},{16,24},{24,32},{32,40},{40,48},{48,56},{56,64},{64,7... | collective-permute-start | bytes 294920 | tf_op jit(solution)/shard_map/ppermute | solution.py:23
  24.6 7.3 %collective-permute-start.1 = (bf16[384,128]{1,0:T(8,128)(2,1)S(1)}, bf16[384,128]{1,0:T(8,128)(2,1)S(1)}, u32[]{:S(2)}, u32[]{:S(2)}) collective-permute-start(bf16[384,128]{1,0:T(8,128)(2,1)S(1)} %collective-permute-done), channel_id=1, source_target_pairs={{0,8},{8,16},{16,24},{24,32},{32,40},{40,48},{48,56},{56,64},{64,7... | collective-permute-start | bytes 294920 | tf_op jit(solution)/shard_map/ppermute | solution.py:23
  31.8 15.7 %copy-start.5 = (bf16[384,128]{1,0:T(8,128)(2,1)}, bf16[384,128]{1,0:T(8,128)(2,1)S(1)}, u32[]{:S(2)}) copy-start(bf16[384,128]{1,0:T(8,128)(2,1)S(1)} %collective-permute-done.1) | copy-start | bytes 294916
  32.1 25.8 %copy-start.7 = (bf16[384,128]{1,0:T(8,128)(2,1)}, bf16[384,128]{1,0:T(8,128)(2,1)S(1)}, u32[]{:S(2)}) copy-start(bf16[384,128]{1,0:T(8,128)(2,1)S(1)} %collective-permute-done.7) | copy-start | bytes 294916
  32.1 10.9 %collective-permute-start.8 = (bf16[384,128]{1,0:T(8,128)(2,1)S(1)}, bf16[384,128]{1,0:T(8,128)(2,1)S(1)}, u32[]{:S(2)}, u32[]{:S(2)}) collective-permute-start(bf16[384,128]{1,0:T(8,128)(2,1)S(1)} %collective-permute-done.7), channel_id=1, source_target_pairs={{0,8},{8,16},{16,24},{24,32},{32,40},{40,48},{48,56},{56,64},{64,7... | collective-permute-start | bytes 294920 | tf_op jit(solution)/shard_map/ppermute | solution.py:23
  37.9 9.8 %collective-permute-start.2 = (bf16[384,128]{1,0:T(8,128)(2,1)S(1)}, bf16[384,128]{1,0:T(8,128)(2,1)}, u32[]{:S(2)}, u32[]{:S(2)}) collective-permute-start(bf16[384,128]{1,0:T(8,128)(2,1)S(1)} %collective-permute-done.1), channel_id=1, source_target_pairs={{0,8},{8,16},{16,24},{24,32},{32,40},{40,48},{48,56},{56,64},{64,7... | collective-permute-start | bytes 294920 | tf_op jit(solution)/shard_map/ppermute | solution.py:23
  43.0 14.8 %copy-start.11 = (bf16[384,128]{1,0:T(8,128)(2,1)}, bf16[384,128]{1,0:T(8,128)(2,1)S(1)}, u32[]{:S(2)}) copy-start(bf16[384,128]{1,0:T(8,128)(2,1)S(1)} %collective-permute-done.8) | copy-start | bytes 294916
  43.0 10.4 %collective-permute-start.9 = (bf16[384,128]{1,0:T(8,128)(2,1)S(1)}, bf16[384,128]{1,0:T(8,128)(2,1)}, u32[]{:S(2)}, u32[]{:S(2)}) collective-permute-start(bf16[384,128]{1,0:T(8,128)(2,1)S(1)} %collective-permute-done.8), channel_id=1, source_target_pairs={{0,8},{8,16},{16,24},{24,32},{32,40},{40,48},{48,56},{56,64},{64,7... | collective-permute-start | bytes 294920 | tf_op jit(solution)/shard_map/ppermute | solution.py:23
  47.7 11.0 %collective-permute-start.3 = (bf16[384,128]{1,0:T(8,128)(2,1)}, bf16[384,128]{1,0:T(8,128)(2,1)}, u32[]{:S(2)}, u32[]{:S(2)}) collective-permute-start(bf16[384,128]{1,0:T(8,128)(2,1)} %collective-permute-done.2), channel_id=1, source_target_pairs={{0,8},{8,16},{16,24},{24,32},{32,40},{40,48},{48,56},{56,64},{64,7... | collective-permute-start | bytes 294920 | tf_op jit(solution)/shard_map/ppermute | solution.py:23
  53.4 9.9 %collective-permute-start.10 = (bf16[384,128]{1,0:T(8,128)(2,1)}, bf16[384,128]{1,0:T(8,128)(2,1)}, u32[]{:S(2)}, u32[]{:S(2)}) collective-permute-start(bf16[384,128]{1,0:T(8,128)(2,1)} %collective-permute-done.9), channel_id=1, source_target_pairs={{0,8},{8,16},{16,24},{24,32},{32,40},{40,48},{48,56},{56,64},{64,7... | collective-permute-start | bytes 294920 | tf_op jit(solution)/shard_map/ppermute | solution.py:23
  58.8 13.1 %collective-permute-start.4 = (bf16[384,128]{1,0:T(8,128)(2,1)}, bf16[384,128]{1,0:T(8,128)(2,1)}, u32[]{:S(2)}, u32[]{:S(2)}) collective-permute-start(bf16[384,128]{1,0:T(8,128)(2,1)} %collective-permute-done.3), channel_id=1, source_target_pairs={{0,8},{8,16},{16,24},{24,32},{32,40},{40,48},{48,56},{56,64},{64,7... | collective-permute-start | bytes 294920 | tf_op jit(solution)/shard_map/ppermute | solution.py:23
  63.3 14.3 %collective-permute-start.11 = (bf16[384,128]{1,0:T(8,128)(2,1)}, bf16[384,128]{1,0:T(8,128)(2,1)}, u32[]{:S(2)}, u32[]{:S(2)}) collective-permute-start(bf16[384,128]{1,0:T(8,128)(2,1)} %collective-permute-done.10), channel_id=1, source_target_pairs={{0,8},{8,16},{16,24},{24,32},{32,40},{40,48},{48,56},{56,64},{64,7... | collective-permute-start | bytes 294920 | tf_op jit(solution)/shard_map/ppermute | solution.py:23
  68.1 12.2 %copy-start.12 = (bf16[384,128]{1,0:T(8,128)(2,1)S(1)}, bf16[384,128]{1,0:T(8,128)(2,1)}, u32[]{:S(2)}) copy-start(bf16[384,128]{1,0:T(8,128)(2,1)} %copy-done.11) | copy-start | bytes 294916
  68.1 12.2 %copy-start.8 = (bf16[384,128]{1,0:T(8,128)(2,1)S(1)}, bf16[384,128]{1,0:T(8,128)(2,1)}, u32[]{:S(2)}) copy-start(bf16[384,128]{1,0:T(8,128)(2,1)} %copy-done.7) | copy-start | bytes 294916
  68.1 12.2 %copy-start.4 = (bf16[384,128]{1,0:T(8,128)(2,1)S(1)}, bf16[384,128]{1,0:T(8,128)(2,1)}, u32[]{:S(2)}) copy-start(bf16[384,128]{1,0:T(8,128)(2,1)} %copy-done.3) | copy-start | bytes 294916
  71.9 9.1 %collective-permute-start.5 = (bf16[384,128]{1,0:T(8,128)(2,1)}, bf16[384,128]{1,0:T(8,128)(2,1)}, u32[]{:S(2)}, u32[]{:S(2)}) collective-permute-start(bf16[384,128]{1,0:T(8,128)(2,1)} %collective-permute-done.4), channel_id=1, source_target_pairs={{0,8},{8,16},{16,24},{24,32},{32,40},{40,48},{48,56},{56,64},{64,7... | collective-permute-start | bytes 294920 | tf_op jit(solution)/shard_map/ppermute | solution.py:23
  80.5 4.1 %copy-start.6 = (bf16[384,128]{1,0:T(8,128)(2,1)S(1)}, bf16[384,128]{1,0:T(8,128)(2,1)}, u32[]{:S(2)}) copy-start(bf16[384,128]{1,0:T(8,128)(2,1)} %copy-done.5) | copy-start | bytes 294916
  89.4 1.6 %copy-start.10 = (f32[3,128,1,2,64]{1,4,3,0,2:T(8,128)S(1)}, f32[3,128,1,2,64]{1,4,3,0,2:T(8,128)}, u32[]{:S(2)}) copy-start(f32[3,128,1,2,64]{1,4,3,0,2:T(8,128)} %copy.226) | copy-start | bytes 589828
  90.8 21.2 %copy-start.16 = (f32[384,2]{0,1:T(2,128)S(1)}, f32[384,2]{0,1:T(2,128)}, u32[]{:S(2)}) copy-start(f32[384,2]{0,1:T(2,128)} %reshape.497) | copy-start | bytes 9220
  90.8 21.2 %copy-start.17 = (f32[384,2]{0,1:T(2,128)S(1)}, f32[384,2]{0,1:T(2,128)}, u32[]{:S(2)}) copy-start(f32[384,2]{0,1:T(2,128)} %reshape.486) | copy-start | bytes 9220
  90.8 21.3 %copy-start.2 = (f32[384,128]{0,1:T(8,128)S(1)}, f32[384,128]{0,1:T(8,128)}, u32[]{:S(2)}) copy-start(f32[384,128]{0,1:T(8,128)} %copy.214) | copy-start | bytes 589828
  90.8 21.3 %copy-start.18 = (f32[128]{0:T(128)S(1)}, f32[128]{0:T(128)}, u32[]{:S(2)}) copy-start(f32[128]{0:T(128)} %param.12) | copy-start | bytes 1540
  92.2 24.6 %all-to-all-start.1 = ((f32[8,1,384]{2,1,0:T(1,128)}), f32[8,1,384]{2,1,0:T(1,128)S(1)}, u32[]{:S(2)}, u32[]{:S(2)}) async-start(f32[8,1,384]{2,1,0:T(1,128)} %broadcast_in_dim.40), calls=%async_computation.1 | async-start | bytes 24576 | tf_op jit(solution)/shard_map/all_to_all | solution.py:28
  116.7 24.9 %all-to-all-start = ((bf16[8,48,2048]{2,1,0:T(8,128)(2,1)}), bf16[8,48,2048]{2,1,0:T(8,128)(2,1)S(1)}, u32[]{:S(2)}, u32[]{:S(2)}) async-start(bf16[8,48,2048]{2,1,0:T(8,128)(2,1)} %bitcast.40), calls=%async_computation | async-start | bytes 3145728 | tf_op jit(solution)/shard_map/all_to_all | solution.py:43
  (4 other events, 6.5 us)
where the time goes:
time: 143 us
  starting transfers between devices  82.6 us (58%)
  waiting for transfers between devices  24.6 us (17%)
  local copies, waits for them, and re-layouts  18.4 us (13%)
  matrix products  10 us (7%)
  other arithmetic  6.14 us (4%)
    ppermute x12, starting transfers between devices, from_behind(): lax.ppermute(value, axis, [(source, source + steps) for source in range(i...  58.5 us
    all_to_all x1, waiting for transfers between devices, sum_at_owner(): lax.all_to_all(tiles, axis, split_axis=0, concat_axis=0, tiled=True)  20.6 us
    all_to_all x1, starting transfers between devices, copy_for_each(): return lax.all_to_all(copies, axis, split_axis=0, concat_axis=0, tiled=True)  19.9 us
    unnamed x54, local copies, waits for them, and re-layouts  6.48 us
    all_to_all x1, starting transfers between devices, sum_at_owner(): lax.all_to_all(tiles, axis, split_axis=0, concat_axis=0, tiled=True)  4.19 us
    dot_general x3, matrix products, band_part(): jnp.einsum('jqchx,jkchx->jchqk', query_blk, key_blk, preferred_element_ty...  3.9 us
    another operation x7, local copies, waits for them, and re-layouts  3.49 us
    dot_general x3, matrix products, project(): jnp.dot(scaled, weight, preferred_element_type=jnp.float32)  2.89 us
  transfers between devices with their start and end apart: 14, of which 3 were waited for; matrix products, arithmetic and copies ran while one was open for 12% of the time, Pallas kernels for 0%

commit v1 on v0

v1 whole, which is shorter than its diff:
```python
import functools

import jax
import jax.numpy as jnp
from jax import lax
from jax.experimental import pallas as pl
from jax.experimental.pallas import tpu as pltpu
from jax.sharding import PartitionSpec as P


HEAD_DIM = 64
WINDOW_FIRST = 128
WINDOW_SECOND = 512
DILATION_SECOND = 4
WINDOW_THIRD = 2048
DILATION_THIRD = 16
CLASSES = DILATION_SECOND

EPS = 1e-06
NEG = -1e30


VMEM = pltpu.VMEM
F32 = jnp.float32
BF16 = jnp.bfloat16


def qkv_kernel(
    chunks, tok_hbm, gain_hbm, wq_hbm, wk_hbm, wv_hbm, q_ref, kv_ref, tok, gain_ref, w, acc, gain_sem, tok_sem, w_sem
):
    rows, depth = tok_hbm.shape
    width = wq_hbm.shape[1]
    piece = depth // chunks
    gain_copy = pltpu.make_async_copy(gain_hbm, gain_ref, gain_sem)
    gain_copy.start()
    copies = []
    for n in range(chunks):
        span = pl.ds(n * piece, piece)
        pair = [pltpu.make_async_copy(tok_hbm.at[:, span], tok.at[:, span], tok_sem.at[n])]
        for m, part in enumerate((wq_hbm, wk_hbm, wv_hbm)):
            pair.append(
                pltpu.make_async_copy(
                    part.at[span, :], w.at[span, pl.ds(m * width, width)], w_sem.at[n, m]
                )
            )
        for copy in pair:
            copy.start()
        copies.append(pair)
    gain_copy.wait()
    squares = jnp.zeros((rows, 128), F32)
    total = jnp.zeros((rows, 3 * width), F32)
    for n in range(chunks):
        for copy in copies[n]:
            copy.wait()
        block = tok[:, n * piece : (n + 1) * piece].astype(F32)
        for lane in range(0, piece, 128):
            part = block[:, lane : lane + 128]
            squares = squares + part * part
        scaled = (block * gain_ref[:, n * piece : (n + 1) * piece]).astype(BF16)
        total = total + jnp.dot(scaled, w[n * piece : (n + 1) * piece, :], preferred_element_type=F32)
    inverse = lax.rsqrt(jnp.sum(squares, axis=-1, keepdims=True) / depth + EPS)
    total = total * inverse
    for m in range(3):
        acc[m] = total[:, m * width : (m + 1) * width]
    share = rows // CLASSES
    for c in range(CLASSES):
        mine = [acc[m, pl.ds(c, share, stride=CLASSES), :] for m in range(3)]
        q_ref[c] = (mine[0] * HEAD_DIM ** (-0.5)).astype(BF16)
        kv_ref[c, :, 0:width] = mine[1].astype(BF16)
        kv_ref[c, :, width : 2 * width] = mine[2].astype(BF16)


def hbm(value):
    return pltpu.with_memory_space_constraint(value, pltpu.HBM)


def qkv(tokens, norm_gain, w_query, w_key, w_value):
    rows, depth = tokens.shape
    width = w_query.shape[1]
    chunks = 4
    share = rows // CLASSES
    return pl.pallas_call(
        functools.partial(qkv_kernel, chunks),
        out_shape=(
            jax.ShapeDtypeStruct((CLASSES, share, width), BF16),
            jax.ShapeDtypeStruct((CLASSES, share, 2 * width), BF16),
        ),
        in_specs=[
            pl.BlockSpec(memory_space=pltpu.HBM),
        ]
        * 5,
        out_specs=(pl.BlockSpec(memory_space=VMEM), pl.BlockSpec(memory_space=VMEM)),
        scratch_shapes=[
            VMEM((rows, depth), BF16),
            VMEM((1, depth), F32),
            VMEM((depth, 3 * width), BF16),
            VMEM((3, rows, width), F32),
            pltpu.SemaphoreType.DMA,
            pltpu.SemaphoreType.DMA((chunks,)),
            pltpu.SemaphoreType.DMA((chunks, 3)),
        ],
        compiler_params=pltpu.CompilerParams(vmem_limit_bytes=20 << 20),
        name="qkv",
    )(hbm(tokens), hbm(norm_gain.reshape(1, depth)), hbm(w_query), hbm(w_key), hbm(w_value))


def attend_kernel(sp_ref, q_ref, own, *rest):
    older = rest[:-4]
    out_ref, k_all, v_all, natural = rest[-4:]
    width = q_ref.shape[2]
    share = q_ref.shape[1]
    far = WINDOW_THIRD // CLASSES
    near = WINDOW_FIRST // CLASSES
    span = far + share
    tail = near + share
    start = span
    for block in (own, *older):
        count = block.shape[1]
        start -= count
        for c in range(CLASSES):
            k_all[c, start : start + count, :] = block[c, :, 0:width]
            v_all[c, start : start + count, :] = block[c, :, width : 2 * width]
    sp = sp_ref[0]
    row = lax.broadcasted_iota(jnp.int32, (share, span), 0)
    col = lax.broadcasted_iota(jnp.int32, (share, span), 1)
    lag = row - col + far
    ratio = DILATION_THIRD // CLASSES
    behind = (lag >= 0).astype(F32)
    count = behind * (
        (lag <= WINDOW_FIRST // CLASSES).astype(F32)
        + (lag <= WINDOW_SECOND // CLASSES).astype(F32)
        + jnp.logical_and(lag <= far, lax.rem(lag + ratio * span, ratio) == 0).astype(F32)
    )
    live = jnp.logical_and(count > 0.5, col >= far - share * sp)
    weight = jnp.where(count > 2.5, jnp.log(F32(3.0)), jnp.where(count > 1.5, jnp.log(F32(2.0)), F32(0.0)))
    bias = jnp.where(live, weight, NEG)
    bias = jnp.concatenate([bias, bias], axis=0)
    row = lax.broadcasted_iota(jnp.int32, (share, tail), 0)
    col = lax.broadcasted_iota(jnp.int32, (share, tail), 1)
    lag = row - col + near
    there = col >= near - share * sp
    after = jnp.where(jnp.logical_and(there, jnp.logical_and(lag >= 0, lag < near)), F32(0.0), NEG)
    before = jnp.where(jnp.logical_and(there, jnp.logical_and(lag >= 1, lag <= near)), F32(0.0), NEG)
    after = jnp.concatenate([after, after], axis=0)
    before = jnp.concatenate([before, before], axis=0)
    lane = lax.broadcasted_iota(jnp.int32, (share, width), 1)
    contract = (((1,), (1,)), ((), ()))
    for c in range(CLASSES):
        query = q_ref[c]
        zero = jnp.zeros_like(query)
        stacked = jnp.concatenate(
            [jnp.where(lane < HEAD_DIM, query, zero), jnp.where(lane < HEAD_DIM, zero, query)], axis=0
        )
        scores = [lax.dot_general(stacked, k_all[c], contract, preferred_element_type=F32) + bias]
        values = [v_all[c]]
        for other in range(CLASSES):
            if other != c:
                part = lax.dot_general(
                    stacked, k_all[other, span - tail : span, :], contract, preferred_element_type=F32
                )
                scores.append(part + (after if c > other else before))
                values.append(v_all[other, span - tail : span, :])
        top = functools.reduce(jnp.maximum, [jnp.max(part, axis=-1, keepdims=True) for part in scores])
        weights = [jnp.exp(part - top) for part in scores]
        norm = functools.reduce(jnp.add, [jnp.sum(part, axis=-1, keepdims=True) for part in weights])
        mixed = functools.reduce(
            jnp.add,
            [
                jnp.dot(part.astype(BF16), value, preferred_element_type=F32)
                for part, value in zip(weights, values)
            ],
        )
        mixed = mixed / norm
        natural[pl.ds(c, share, stride=CLASSES), :] = jnp.where(lane < HEAD_DIM, mixed[:share], mixed[share:])
    out_ref[...] = natural[...].astype(BF16)


def attend(sp, query, own, older):
    share, width = query.shape[1:]
    span = WINDOW_THIRD // CLASSES + share
    return pl.pallas_call(
        attend_kernel,
        out_shape=jax.ShapeDtypeStruct((CLASSES * share, width), BF16),
        in_specs=[pl.BlockSpec(memory_space=pltpu.SMEM)]
        + [pl.BlockSpec(memory_space=VMEM)] * (2 + len(older)),
        out_specs=pl.BlockSpec(memory_space=VMEM),
        scratch_shapes=[
            VMEM((CLASSES, span, width), BF16),
            VMEM((CLASSES, span, width), BF16),
            VMEM((CLASSES * share, width), F32),
        ],
        compiler_params=pltpu.CompilerParams(vmem_limit_bytes=20 << 20),
        name="attend",
    )(sp, query, own, *older)


def project_kernel(tp_ref, att_ref, mine, partner, out_ref):
    count, rows, width = att_ref.shape
    tp = tp_ref[0]
    squares = jnp.zeros((rows, width), F32)
    for n in range(count):
        part = att_ref[n].astype(F32)
        squares = squares + part * part
    scale = lax.rsqrt(jnp.sum(squares, axis=-1, keepdims=True) / (count * width) + EPS)
    total = None
    for other, weights in ((0, mine), (1, partner)):
        places = [lax.rem(lax.bitwise_xor(tp, other) + step + count, count) for step in (0, -2, 2, 4)]
        left = jnp.concatenate([att_ref[place] for place in places], axis=1)
        part = jnp.dot(left, weights[...], preferred_element_type=F32)
        total = part if total is None else total + part
    out_ref[...] = (total * scale).astype(BF16)


def project(tp, attended, mine, partner):
    rows = attended.shape[1]
    return pl.pallas_call(
        project_kernel,
        out_shape=jax.ShapeDtypeStruct((rows, mine.shape[1]), BF16),
        in_specs=[pl.BlockSpec(memory_space=pltpu.SMEM)] + [pl.BlockSpec(memory_space=VMEM)] * 3,
        out_specs=pl.BlockSpec(memory_space=VMEM),
        compiler_params=pltpu.CompilerParams(vmem_limit_bytes=20 << 20),
        name="project",
    )(tp, attended, mine, partner)


def ahead(value, steps, first):
    count = lax.axis_size("sp")
    return lax.ppermute(value, "sp", [(source, source + steps) for source in range(first, count - steps)])


def across(value, pairs):
    return lax.ppermute(value, "tp", pairs)


def layer(tokens, norm_gain, w_query, w_key, w_value, out_gain, w_out):
    tok_rows = tokens.shape[0]
    sp = lax.axis_index("sp").astype(jnp.int32).reshape(1)
    tp = lax.axis_index("tp").astype(jnp.int32).reshape(1)
    n_tp = lax.axis_size("tp")
    query, own = qkv(tokens, norm_gain, w_query, w_key, w_value)

    one = ahead(own, 1, 0)
    two = ahead(own, 2, 0)
    three = ahead(one, 2, 1)
    four = ahead(two, 2, 2)
    five = ahead(three, 2, 3)
    excess = 6 * (tok_rows // CLASSES) - WINDOW_THIRD // CLASSES
    six = ahead(four[:, excess:, :], 2, 4)

    scaled_out = (w_out.astype(F32) * out_gain[:, None]).astype(BF16)
    up = [(n, (n + 2) % n_tp) for n in range(n_tp)]
    down = [(n, (n - 2) % n_tp) for n in range(n_tp)]
    swap = [(n, n ^ 1) for n in range(n_tp)]
    half = w_out.shape[0] // 2
    behind = across(scaled_out, up)
    front = across(scaled_out, down)
    far_low = across(behind[:half], up)
    far_high = across(front[half:], down)
    mine = jnp.concatenate([scaled_out, behind, front, far_low, far_high], axis=0)
    partner = across(mine, swap)

    attended = attend(sp, query, own, (one, two, three, four, five, six))
    tiles = attended.reshape(n_tp, tok_rows // n_tp, -1)
    arrived = lax.all_to_all(tiles, "tp", split_axis=0, concat_axis=0, tiled=True)
    return project(tp, arrived, mine, partner)


def solution(mesh):
    in_specs = (
        P(("grp", "sp"), None),
        P(),
        P(None, "tp"),
        P(None, "tp"),
        P(None, "tp"),
        P("tp"),
        P("tp", None),
    )
    out_specs = P(("grp", "sp", "tp"), None)
    return jax.shard_map(layer, mesh=mesh, in_specs=in_specs, out_specs=out_specs, check_vma=False)
```

time: 143 us -> 107 us (0.75)
  the two profiles are of different devices: /device:TPU:33 before, /device:TPU:744 now
where the time goes in v1:
time: 107 us; the launch traced here: 106 us
  starting transfers between devices  72.2 us (67%)
  waiting for transfers between devices  23.5 us (22%)
  Pallas kernels  9.17 us (9%)
  other arithmetic  1.21 us (1%)
    ppermute x6, starting transfers between devices, ahead(): lax.ppermute(value, 'sp', [(source, source + steps) for source in range(f...  51 us
    ppermute x5, starting transfers between devices, across(): return lax.ppermute(value, 'tp', pairs)  16.2 us
    ppermute x5, waiting for transfers between devices, across(): return lax.ppermute(value, 'tp', pairs)  14.5 us
    all_to_all x1, waiting for transfers between devices, layer(): lax.all_to_all(tiles, 'tp', split_axis=0, concat_axis=0, tiled=True)  5.8 us
    all_to_all x1, starting transfers between devices, layer(): lax.all_to_all(tiles, 'tp', split_axis=0, concat_axis=0, tiled=True)  4.99 us
    ppermute x6, waiting for transfers between devices, ahead(): lax.ppermute(value, 'sp', [(source, source + steps) for source in range(f...  3.18 us
    pallas_call x1, Pallas kernels, qkv(): pl.pallas_call(functools.partial(qkv_kernel, chunks), out_shape=(jax.Shap...  3.17 us
    pallas_call x1, Pallas kernels, project(): pl.pallas_call(project_kernel, out_shape=jax.ShapeDtypeStruct((rows, mine...  3.11 us
  transfers between devices with their start and end apart: 12, of which 6 were waited for; matrix products, arithmetic and copies ran while one was open for 0% of the time, Pallas kernels for 6%

profile of v1, /device:TPU:744, one launch (start us, length us, event | category | flops | bytes accessed | tf_op | source)
XLA Modules:
  0.0 106.4 jit_solution(5984671505488902152)
XLA Ops:
  0.0 1.2 %constant_dynamic-update-slice_fusion.4 = (bf16[512,2048]{1,0:T(8,128)(2,1)S(1)}, bf16[128,2048]{1,0:T(8,128)(2,1)S(1)}) fusion(f32[128]{0:T(128)} %param.12, bf16[128,2048]{1,0:T(8,128)(2,1)} %param.13), kind=kLoop, calls=%fused_computation.5 | loop fusion | flops 786431 | bytes 1573376
  1.2 3.6 %collective-permute-start.6 = (bf16[128,2048]{1,0:T(8,128)(2,1)S(1)}, bf16[128,2048]{1,0:T(8,128)(2,1)S(1)}, u32[]{:S(2)}, u32[]{:S(2)}) collective-permute-start(bf16[128,2048]{1,0:T(8,128)(2,1)S(1)} %get-tuple-element.10), channel_id=1, source_target_pairs={{0,2},{1,3},{2,4},{3,5},{4,6},{5,7},{6,0},{7,1},{8,10},{9,11},{10,... | collective-permute-start | bytes 1572872 | tf_op jit(solution)/shard_map/ppermute | solution.py:232
  4.8 3.5 %collective-permute-start.7 = (bf16[128,2048]{1,0:T(8,128)(2,1)S(1)}, bf16[128,2048]{1,0:T(8,128)(2,1)S(1)}, u32[]{:S(2)}, u32[]{:S(2)}) collective-permute-start(bf16[128,2048]{1,0:T(8,128)(2,1)S(1)} %get-tuple-element.10), channel_id=1, source_target_pairs={{0,6},{1,7},{2,0},{3,1},{4,2},{5,3},{6,4},{7,5},{8,14},{9,15},{10,... | collective-permute-start | bytes 1572872 | tf_op jit(solution)/shard_map/ppermute | solution.py:232
  8.3 10.0 %collective-permute-done.6 = bf16[128,2048]{1,0:T(8,128)(2,1)S(1)} collective-permute-done((bf16[128,2048]{1,0:T(8,128)(2,1)S(1)}, bf16[128,2048]{1,0:T(8,128)(2,1)S(1)}, u32[]{:S(2)}, u32[]{:S(2)}) %collective-permute-start.6) | collective-permute-done | bytes 524320 | tf_op jit(solution)/shard_map/ppermute | solution.py:232
  18.3 2.1 %collective-permute-start.8 = (bf16[64,2048]{1,0:T(8,128)(2,1)S(1)}, bf16[64,2048]{1,0:T(8,128)(2,1)S(1)}, u32[]{:S(2)}, u32[]{:S(2)}) collective-permute-start(bf16[64,2048]{1,0:T(8,128)(2,1)S(1)} %slice.13), channel_id=1, source_target_pairs={{0,2},{1,3},{2,4},{3,5},{4,6},{5,7},{6,0},{7,1},{8,10},{9,11},{10,... | collective-permute-start | bytes 786440 | tf_op jit(solution)/shard_map/ppermute | solution.py:232
  20.5 0.0 collective-permute-done.7
  20.5 5.0 %collective-permute-start.9 = (bf16[64,2048]{1,0:T(8,128)(2,1)S(1)}, bf16[64,2048]{1,0:T(8,128)(2,1)S(1)}, u32[]{:S(2)}, u32[]{:S(2)}) collective-permute-start(bf16[64,2048]{1,0:T(8,128)(2,1)S(1)} %slice.14), channel_id=1, source_target_pairs={{0,6},{1,7},{2,0},{3,1},{4,2},{5,3},{6,4},{7,5},{8,14},{9,15},{10,... | collective-permute-start | bytes 786440 | tf_op jit(solution)/shard_map/ppermute | solution.py:232
  25.6 3.4 %collective-permute-done.8 = bf16[64,2048]{1,0:T(8,128)(2,1)S(1)} collective-permute-done((bf16[64,2048]{1,0:T(8,128)(2,1)S(1)}, bf16[64,2048]{1,0:T(8,128)(2,1)S(1)}, u32[]{:S(2)}, u32[]{:S(2)}) %collective-permute-start.8) | collective-permute-done | bytes 262176 | tf_op jit(solution)/shard_map/ppermute | solution.py:232
  29.0 1.2 %collective-permute-done.9 = bf16[64,2048]{1,0:T(8,128)(2,1)S(1)} collective-permute-done((bf16[64,2048]{1,0:T(8,128)(2,1)S(1)}, bf16[64,2048]{1,0:T(8,128)(2,1)S(1)}, u32[]{:S(2)}, u32[]{:S(2)}) %collective-permute-start.9) | collective-permute-done | bytes 262176 | tf_op jit(solution)/shard_map/ppermute | solution.py:232
  30.2 2.0 %collective-permute-start.10 = (bf16[512,2048]{1,0:T(8,128)(2,1)S(1)}, bf16[512,2048]{1,0:T(8,128)(2,1)}, u32[]{:S(2)}, u32[]{:S(2)}) collective-permute-start(bf16[512,2048]{1,0:T(8,128)(2,1)S(1)} %constant_dynamic-update-slice_fusion.mine), channel_id=1, source_target_pairs={{0,1},{1,0},{2,3},{3,2},{4,5},{5,4},{6,7},{7,6},{8,9},{9,8},{10,11... | collective-permute-start | bytes 6291464 | tf_op jit(solution)/shard_map/ppermute | solution.py:232
  32.2 3.2 %qkv.1 = (bf16[4,96,128]{2,1,0:T(8,128)(2,1)S(1)}, bf16[4,96,256]{2,1,0:T(8,128)(2,1)S(1)}) custom-call(bf16[384,2048]{1,0:T(8,128)(2,1)} %tok_hbm.1, f32[1,2048]{1,0:T(1,128)} %bitcast.4, bf16[2048,128]{1,0:T(8,128)(2,1)} %wq_hbm.1, bf16[2048,128]{1,0:T(8,128)(2,1)} %wk_hbm.1, bf16[2048,128]{1,0:T(8,128)(2,1)} %wv_hbm.1), custom_call_target="tpu_custom_call" | custom-call | tf_op jit(solution)/shard_map/qkv/pallas_call | solution.py:82
  35.3 5.9 %collective-permute-start = (bf16[4,96,256]{2,1,0:T(8,128)(2,1)S(1)}, bf16[4,96,256]{2,1,0:T(8,128)(2,1)S(1)}, u32[]{:S(2)}, u32[]{:S(2)}) collective-permute-start(bf16[4,96,256]{2,1,0:T(8,128)(2,1)S(1)} %get-tuple-element.8.own), channel_id=1, source_target_pairs={{0,8},{8,16},{16,24},{24,32},{32,40},{40,48},{48,56},{56,64},{64,7... | collective-permute-start | bytes 589832 | tf_op jit(solution)/shard_map/ppermute | solution.py:228
  41.3 6.9 %collective-permute-start.1 = (bf16[4,96,256]{2,1,0:T(8,128)(2,1)S(1)}, bf16[4,96,256]{2,1,0:T(8,128)(2,1)S(1)}, u32[]{:S(2)}, u32[]{:S(2)}) collective-permute-start(bf16[4,96,256]{2,1,0:T(8,128)(2,1)S(1)} %get-tuple-element.8.own), channel_id=1, source_target_pairs={{0,16},{8,24},{16,32},{24,40},{32,48},{40,56},{48,64},{56,72},{64,... | collective-permute-start | bytes 589832 | tf_op jit(solution)/shard_map/ppermute | solution.py:228
  48.2 0.0 collective-permute-done.rest_0_
  48.2 8.1 %collective-permute-start.2 = (bf16[4,96,256]{2,1,0:T(8,128)(2,1)S(1)}, bf16[4,96,256]{2,1,0:T(8,128)(2,1)S(1)}, u32[]{:S(2)}, u32[]{:S(2)}) collective-permute-start(bf16[4,96,256]{2,1,0:T(8,128)(2,1)S(1)} %collective-permute-done.rest_0_), channel_id=1, source_target_pairs={{8,24},{16,32},{24,40},{32,48},{40,56},{48,64},{56,72},{64,80},{72... | collective-permute-start | bytes 589832 | tf_op jit(solution)/shard_map/ppermute | solution.py:228
  56.4 0.0 collective-permute-done.1.rest_1_
  56.4 10.8 %collective-permute-start.3 = (bf16[4,96,256]{2,1,0:T(8,128)(2,1)S(1)}, bf16[4,96,256]{2,1,0:T(8,128)(2,1)S(1)}, u32[]{:S(2)}, u32[]{:S(2)}) collective-permute-start(bf16[4,96,256]{2,1,0:T(8,128)(2,1)S(1)} %collective-permute-done.1.rest_1_), channel_id=1, source_target_pairs={{16,32},{24,40},{32,48},{40,56},{48,64},{56,72},{64,80},{72,88},{8... | collective-permute-start | bytes 589832 | tf_op jit(solution)/shard_map/ppermute | solution.py:228
  67.2 0.0 collective-permute-done.2.rest_2_
  67.2 10.7 %collective-permute-start.4 = (bf16[4,96,256]{2,1,0:T(8,128)(2,1)S(1)}, bf16[4,96,256]{2,1,0:T(8,128)(2,1)S(1)}, u32[]{:S(2)}, u32[]{:S(2)}) collective-permute-start(bf16[4,96,256]{2,1,0:T(8,128)(2,1)S(1)} %collective-permute-done.2.rest_2_), channel_id=1, source_target_pairs={{24,40},{32,48},{40,56},{48,64},{56,72},{64,80},{72,88},{80,96},{8... | collective-permute-start | bytes 589832 | tf_op jit(solution)/shard_map/ppermute | solution.py:228
  78.0 1.3 %collective-permute-done.3.rest_3_ = bf16[4,96,256]{2,1,0:T(8,128)(2,1)S(1)} collective-permute-done((bf16[4,96,256]{2,1,0:T(8,128)(2,1)S(1)}, bf16[4,96,256]{2,1,0:T(8,128)(2,1)S(1)}, u32[]{:S(2)}, u32[]{:S(2)}) %collective-permute-start.3) | collective-permute-done | bytes 196640 | tf_op jit(solution)/shard_map/ppermute | solution.py:228
  79.3 8.5 %collective-permute-start.5 = (bf16[4,32,256]{2,1,0:T(8,128)(2,1)S(1)}, bf16[4,32,256]{2,1,0:T(8,128)(2,1)S(1)}, u32[]{:S(2)}, u32[]{:S(2)}) collective-permute-start(bf16[4,32,256]{2,1,0:T(8,128)(2,1)S(1)} %slice.12), channel_id=1, source_target_pairs={{32,48},{40,56},{48,64},{56,72},{64,80},{72,88},{80,96},{88,104},{... | collective-permute-start | bytes 196616 | tf_op jit(solution)/shard_map/ppermute | solution.py:228
  87.8 1.9 %collective-permute-done.5.rest_5_ = bf16[4,32,256]{2,1,0:T(8,128)(2,1)S(1)} collective-permute-done((bf16[4,32,256]{2,1,0:T(8,128)(2,1)S(1)}, bf16[4,32,256]{2,1,0:T(8,128)(2,1)S(1)}, u32[]{:S(2)}, u32[]{:S(2)}) %collective-permute-start.5) | collective-permute-done | bytes 65568 | tf_op jit(solution)/shard_map/ppermute | solution.py:228
  89.6 0.0 collective-permute-done.4.rest_4_
  89.6 2.9 %attend.1 = bf16[384,128]{1,0:T(8,128)(2,1)} custom-call(s32[1]{0:T(128)} %bitcast.1.sp_ref, bf16[4,96,128]{2,1,0:T(8,128)(2,1)S(1)} %get-tuple-element.7.q_ref, bf16[4,96,256]{2,1,0:T(8,128)(2,1)S(1)} %get-tuple-element.8.own, bf16[4,96,256]{2,1,0:T(8,128)(2,1)S(1)} %collective-permute-done.rest_0_, bf16[4,96,256]{2,1,0:T(8,128)(2,1)S(1)} %collective-permute-done.1.rest_1_, ...), custom_call_target="tpu_custom_call" | custom-call | tf_op jit(solution)/shard_map/attend/pallas_call | solution.py:181
  92.5 5.0 %all-to-all-start = ((bf16[8,48,128]{2,1,0:T(8,128)(2,1)}), bf16[8,48,128]{2,1,0:T(8,128)(2,1)S(1)}, u32[]{:S(2)}, u32[]{:S(2)}) async-start(bf16[8,48,128]{2,1,0:T(8,128)(2,1)} %bitcast.3), calls=%async_computation | async-start | bytes 196608 | tf_op jit(solution)/shard_map/all_to_all | solution.py:264
  97.5 5.8 %all-to-all-done.att_ref = bf16[8,48,128]{2,1,0:T(8,128)(2,1)S(1)} async-done(((bf16[8,48,128]{2,1,0:T(8,128)(2,1)}), bf16[8,48,128]{2,1,0:T(8,128)(2,1)S(1)}, u32[]{:S(2)}, u32[]{:S(2)}) %all-to-all-start) | async-done | bytes 98336 | tf_op jit(solution)/shard_map/all_to_all | solution.py:264
  103.3 0.0 collective-permute-done.10.partner
  103.3 3.1 %project.1 = bf16[48,2048]{1,0:T(8,128)(2,1)} custom-call(s32[1]{0:T(128)} %bitcast.tp_ref, bf16[8,48,128]{2,1,0:T(8,128)(2,1)S(1)} %all-to-all-done.att_ref, bf16[512,2048]{1,0:T(8,128)(2,1)S(1)} %constant_dynamic-update-slice_fusion.mine, bf16[512,2048]{1,0:T(8,128)(2,1)} %collective-permute-done.10.partner), custom_call_target="tpu_custom_call" | custom-call | tf_op jit(solution)/shard_map/project/pallas_call | solution.py:216
  (7 shorter events, 0.2 us)
Async XLA Ops:
  1.2 17.1 %collective-permute-start.6 = (bf16[128,2048]{1,0:T(8,128)(2,1)S(1)}, bf16[128,2048]{1,0:T(8,128)(2,1)S(1)}, u32[]{:S(2)}, u32[]{:S(2)}) collective-permute-start(bf16[128,2048]{1,0:T(8,128)(2,1)S(1)} %get-tuple-element.10), channel_id=1, source_target_pairs={{0,2},{1,3},{2,4},{3,5},{4,6},{5,7},{6,0},{7,1},{8,10},{9,11},{10,... | collective-permute-start | bytes 1572872 | tf_op jit(solution)/shard_map/ppermute | solution.py:232
  4.8 15.7 %collective-permute-start.7 = (bf16[128,2048]{1,0:T(8,128)(2,1)S(1)}, bf16[128,2048]{1,0:T(8,128)(2,1)S(1)}, u32[]{:S(2)}, u32[]{:S(2)}) collective-permute-start(bf16[128,2048]{1,0:T(8,128)(2,1)S(1)} %get-tuple-element.10), channel_id=1, source_target_pairs={{0,6},{1,7},{2,0},{3,1},{4,2},{5,3},{6,4},{7,5},{8,14},{9,15},{10,... | collective-permute-start | bytes 1572872 | tf_op jit(solution)/shard_map/ppermute | solution.py:232
  18.3 10.6 %collective-permute-start.8 = (bf16[64,2048]{1,0:T(8,128)(2,1)S(1)}, bf16[64,2048]{1,0:T(8,128)(2,1)S(1)}, u32[]{:S(2)}, u32[]{:S(2)}) collective-permute-start(bf16[64,2048]{1,0:T(8,128)(2,1)S(1)} %slice.13), channel_id=1, source_target_pairs={{0,2},{1,3},{2,4},{3,5},{4,6},{5,7},{6,0},{7,1},{8,10},{9,11},{10,... | collective-permute-start | bytes 786440 | tf_op jit(solution)/shard_map/ppermute | solution.py:232
  20.5 9.7 %collective-permute-start.9 = (bf16[64,2048]{1,0:T(8,128)(2,1)S(1)}, bf16[64,2048]{1,0:T(8,128)(2,1)S(1)}, u32[]{:S(2)}, u32[]{:S(2)}) collective-permute-start(bf16[64,2048]{1,0:T(8,128)(2,1)S(1)} %slice.14), channel_id=1, source_target_pairs={{0,6},{1,7},{2,0},{3,1},{4,2},{5,3},{6,4},{7,5},{8,14},{9,15},{10,... | collective-permute-start | bytes 786440 | tf_op jit(solution)/shard_map/ppermute | solution.py:232
  30.2 73.1 %collective-permute-start.10 = (bf16[512,2048]{1,0:T(8,128)(2,1)S(1)}, bf16[512,2048]{1,0:T(8,128)(2,1)}, u32[]{:S(2)}, u32[]{:S(2)}) collective-permute-start(bf16[512,2048]{1,0:T(8,128)(2,1)S(1)} %constant_dynamic-update-slice_fusion.mine), channel_id=1, source_target_pairs={{0,1},{1,0},{2,3},{3,2},{4,5},{5,4},{6,7},{7,6},{8,9},{9,8},{10,11... | collective-permute-start | bytes 6291464 | tf_op jit(solution)/shard_map/ppermute | solution.py:232
  35.3 12.9 %collective-permute-start = (bf16[4,96,256]{2,1,0:T(8,128)(2,1)S(1)}, bf16[4,96,256]{2,1,0:T(8,128)(2,1)S(1)}, u32[]{:S(2)}, u32[]{:S(2)}) collective-permute-start(bf16[4,96,256]{2,1,0:T(8,128)(2,1)S(1)} %get-tuple-element.8.own), channel_id=1, source_target_pairs={{0,8},{8,16},{16,24},{24,32},{32,40},{40,48},{48,56},{56,64},{64,7... | collective-permute-start | bytes 589832 | tf_op jit(solution)/shard_map/ppermute | solution.py:228
  41.3 15.1 %collective-permute-start.1 = (bf16[4,96,256]{2,1,0:T(8,128)(2,1)S(1)}, bf16[4,96,256]{2,1,0:T(8,128)(2,1)S(1)}, u32[]{:S(2)}, u32[]{:S(2)}) collective-permute-start(bf16[4,96,256]{2,1,0:T(8,128)(2,1)S(1)} %get-tuple-element.8.own), channel_id=1, source_target_pairs={{0,16},{8,24},{16,32},{24,40},{32,48},{40,56},{48,64},{56,72},{64,... | collective-permute-start | bytes 589832 | tf_op jit(solution)/shard_map/ppermute | solution.py:228
  48.2 19.0 %collective-permute-start.2 = (bf16[4,96,256]{2,1,0:T(8,128)(2,1)S(1)}, bf16[4,96,256]{2,1,0:T(8,128)(2,1)S(1)}, u32[]{:S(2)}, u32[]{:S(2)}) collective-permute-start(bf16[4,96,256]{2,1,0:T(8,128)(2,1)S(1)} %collective-permute-done.rest_0_), channel_id=1, source_target_pairs={{8,24},{16,32},{24,40},{32,48},{40,56},{48,64},{56,72},{64,80},{72... | collective-permute-start | bytes 589832 | tf_op jit(solution)/shard_map/ppermute | solution.py:228
  56.4 22.9 %collective-permute-start.3 = (bf16[4,96,256]{2,1,0:T(8,128)(2,1)S(1)}, bf16[4,96,256]{2,1,0:T(8,128)(2,1)S(1)}, u32[]{:S(2)}, u32[]{:S(2)}) collective-permute-start(bf16[4,96,256]{2,1,0:T(8,128)(2,1)S(1)} %collective-permute-done.1.rest_1_), channel_id=1, source_target_pairs={{16,32},{24,40},{32,48},{40,56},{48,64},{56,72},{64,80},{72,88},{8... | collective-permute-start | bytes 589832 | tf_op jit(solution)/shard_map/ppermute | solution.py:228
  67.2 22.4 %collective-permute-start.4 = (bf16[4,96,256]{2,1,0:T(8,128)(2,1)S(1)}, bf16[4,96,256]{2,1,0:T(8,128)(2,1)S(1)}, u32[]{:S(2)}, u32[]{:S(2)}) collective-permute-start(bf16[4,96,256]{2,1,0:T(8,128)(2,1)S(1)} %collective-permute-done.2.rest_2_), channel_id=1, source_target_pairs={{24,40},{32,48},{40,56},{48,64},{56,72},{64,80},{72,88},{80,96},{8... | collective-permute-start | bytes 589832 | tf_op jit(solution)/shard_map/ppermute | solution.py:228
  79.3 10.4 %collective-permute-start.5 = (bf16[4,32,256]{2,1,0:T(8,128)(2,1)S(1)}, bf16[4,32,256]{2,1,0:T(8,128)(2,1)S(1)}, u32[]{:S(2)}, u32[]{:S(2)}) collective-permute-start(bf16[4,32,256]{2,1,0:T(8,128)(2,1)S(1)} %slice.12), channel_id=1, source_target_pairs={{32,48},{40,56},{48,64},{56,72},{64,80},{72,88},{80,96},{88,104},{... | collective-permute-start | bytes 196616 | tf_op jit(solution)/shard_map/ppermute | solution.py:228
  92.5 10.8 %all-to-all-start = ((bf16[8,48,128]{2,1,0:T(8,128)(2,1)}), bf16[8,48,128]{2,1,0:T(8,128)(2,1)S(1)}, u32[]{:S(2)}, u32[]{:S(2)}) async-start(bf16[8,48,128]{2,1,0:T(8,128)(2,1)} %bitcast.3), calls=%async_computation | async-start | bytes 196608 | tf_op jit(solution)/shard_map/all_to_all | solution.py:264

commit v2 on v1

--- a/solution.py
+++ b/solution.py
@@ -104,9 +104,20 @@
     )(hbm(tokens), hbm(norm_gain.reshape(1, depth)), hbm(w_query), hbm(w_key), hbm(w_value))
 
 
-def attend_kernel(sp_ref, q_ref, own, *rest):
-    older = rest[:-4]
-    out_ref, k_all, v_all, natural = rest[-4:]
+def split(value, lanes):
+    high = value.astype(BF16)
+    left = value - high.astype(F32)
+    middle = left.astype(BF16)
+    low = (left - middle.astype(F32)).astype(BF16)
+    lane = lax.broadcasted_iota(jnp.int32, (value.shape[0], lanes), 1)
+    zero = jnp.zeros((value.shape[0], lanes), F32)
+    spread = jnp.where(lane == 0, high.astype(F32), jnp.where(lane == 1, middle.astype(F32), jnp.where(lane == 2, low.astype(F32), zero)))
+    return spread.astype(BF16)
+
+
+def attend_kernel(sp_ref, core_ref, q_ref, own, *rest):
+    older = rest[:-6]
+    gain_ref, keep_ref, give_ref, k_all, v_all, natural = rest[-6:]
     width = q_ref.shape[2]
     share = q_ref.shape[1]
     far = WINDOW_THIRD // CLASSES
@@ -172,18 +183,25 @@
         )
         mixed = mixed / norm
         natural[pl.ds(c, share, stride=CLASSES), :] = jnp.where(lane < HEAD_DIM, mixed[:share], mixed[share:])
-    out_ref[...] = natural[...].astype(BF16)
-
-
-def attend(sp, query, own, older):
+    core = core_ref[0]
+    part = keep_ref.shape[1]
+    for side, target in ((core, keep_ref), (1 - core, give_ref)):
+        for place in range(keep_ref.shape[0]):
+            first = pl.multiple_of((2 * place + side) * part, 16)
+            block = natural[pl.ds(first, part), :]
+            target[place, :, 0:width] = (block * gain_ref[...]).astype(BF16)
+            target[place, :, width : 2 * width] = split(jnp.sum(block * block, axis=-1, keepdims=True), width)
+
+
+def attend(sp, core, query, own, older, gain, parts):
     share, width = query.shape[1:]
     span = WINDOW_THIRD // CLASSES + share
     return pl.pallas_call(
         attend_kernel,
-        out_shape=jax.ShapeDtypeStruct((CLASSES * share, width), BF16),
-        in_specs=[pl.BlockSpec(memory_space=pltpu.SMEM)]
-        + [pl.BlockSpec(memory_space=VMEM)] * (2 + len(older)),
-        out_specs=pl.BlockSpec(memory_space=VMEM),
+        out_shape=(jax.ShapeDtypeStruct((parts, CLASSES * share // (2 * parts), 2 * width), BF16),) * 2,
+        in_specs=[pl.BlockSpec(memory_space=pltpu.SMEM)] * 2
+        + [pl.BlockSpec(memory_space=VMEM)] * (3 + len(older)),
+        out_specs=(pl.BlockSpec(memory_space=VMEM),) * 2,
         scratch_shapes=[
             VMEM((CLASSES, span, width), BF16),
             VMEM((CLASSES, span, width), BF16),
@@ -191,36 +209,56 @@
         ],
         compiler_params=pltpu.CompilerParams(vmem_limit_bytes=20 << 20),
         name="attend",
-    )(sp, query, own, *older)
-
-
-def project_kernel(tp_ref, att_ref, mine, partner, out_ref):
-    count, rows, width = att_ref.shape
-    tp = tp_ref[0]
-    squares = jnp.zeros((rows, width), F32)
-    for n in range(count):
-        part = att_ref[n].astype(F32)
-        squares = squares + part * part
-    scale = lax.rsqrt(jnp.sum(squares, axis=-1, keepdims=True) / (count * width) + EPS)
-    total = None
-    for other, weights in ((0, mine), (1, partner)):
-        places = [lax.rem(lax.bitwise_xor(tp, other) + step + count, count) for step in (0, -2, 2, 4)]
-        left = jnp.concatenate([att_ref[place] for place in places], axis=1)
-        part = jnp.dot(left, weights[...], preferred_element_type=F32)
-        total = part if total is None else total + part
-    out_ref[...] = (total * scale).astype(BF16)
-
-
-def project(tp, attended, mine, partner):
-    rows = attended.shape[1]
+    )(sp, core, query, own, *older, gain)
+
+
+def product_kernel(keep_ref, got_ref, mine, partner, out_ref):
+    parts, rows, double = keep_ref.shape
+    width = double // 2
+    columns = mine.shape[1]
+    keep = keep_ref[...].reshape(parts * rows, double)
+    got = got_ref[...].reshape(parts * rows, double)
+    total = jnp.dot(keep[:, :width], mine[...], preferred_element_type=F32)
+    total = total + jnp.dot(got[:, :width], partner[...], preferred_element_type=F32)
+    squares = jnp.sum(keep[:, width:].astype(F32) + got[:, width:].astype(F32), axis=-1, keepdims=True)
+    out_ref[:, :, 0:columns] = total.astype(BF16).reshape(parts, rows, columns)
+    out_ref[:, :, columns : columns + width] = split(squares, width).reshape(parts, rows, width)
+
+
+def product(keep, got, mine, partner):
+    parts, rows, double = keep.shape
     return pl.pallas_call(
-        project_kernel,
-        out_shape=jax.ShapeDtypeStruct((rows, mine.shape[1]), BF16),
-        in_specs=[pl.BlockSpec(memory_space=pltpu.SMEM)] + [pl.BlockSpec(memory_space=VMEM)] * 3,
+        product_kernel,
+        out_shape=jax.ShapeDtypeStruct((parts, rows, mine.shape[1] + double // 2), BF16),
+        in_specs=[pl.BlockSpec(memory_space=VMEM)] * 4,
         out_specs=pl.BlockSpec(memory_space=VMEM),
         compiler_params=pltpu.CompilerParams(vmem_limit_bytes=20 << 20),
-        name="project",
-    )(tp, attended, mine, partner)
+        name="product",
+    )(keep, got, mine, partner)
+
+
+def finish_kernel(channels, parts_ref, out_ref):
+    parts, rows, columns = parts_ref.shape
+    wide = out_ref.shape[1]
+    squares = jnp.zeros((rows, columns - wide), F32)
+    for n in range(parts):
+        squares = squares + parts_ref[n, :, wide:columns].astype(F32)
+    scale = lax.rsqrt(jnp.sum(squares, axis=-1, keepdims=True) / channels + EPS)
+    total = parts_ref[0, :, 0:wide].astype(F32)
+    for n in range(1, parts):
+        total = total + parts_ref[n, :, 0:wide].astype(F32)
+    out_ref[...] = (total * scale).astype(BF16)
+
+
+def finish(arrived, wide, channels):
+    return pl.pallas_call(
+        functools.partial(finish_kernel, channels),
+        out_shape=jax.ShapeDtypeStruct((arrived.shape[1], wide), BF16),
+        in_specs=[pl.BlockSpec(memory_space=VMEM)],
+        out_specs=pl.BlockSpec(memory_space=VMEM),
+        compiler_params=pltpu.CompilerParams(vmem_limit_bytes=20 << 20),
+        name="finish",
+    )(arrived)
 
 
 def ahead(value, steps, first):
@@ -247,22 +285,16 @@
     excess = 6 * (tok_rows // CLASSES) - WINDOW_THIRD // CLASSES
     six = ahead(four[:, excess:, :], 2, 4)
 
-    scaled_out = (w_out.astype(F32) * out_gain[:, None]).astype(BF16)
-    up = [(n, (n + 2) % n_tp) for n in range(n_tp)]
-    down = [(n, (n - 2) % n_tp) for n in range(n_tp)]
     swap = [(n, n ^ 1) for n in range(n_tp)]
-    half = w_out.shape[0] // 2
-    behind = across(scaled_out, up)
-    front = across(scaled_out, down)
-    far_low = across(behind[:half], up)
-    far_high = across(front[half:], down)
-    mine = jnp.concatenate([scaled_out, behind, front, far_low, far_high], axis=0)
-    partner = across(mine, swap)
-
-    attended = attend(sp, query, own, (one, two, three, four, five, six))
-    tiles = attended.reshape(n_tp, tok_rows // n_tp, -1)
-    arrived = lax.all_to_all(tiles, "tp", split_axis=0, concat_axis=0, tiled=True)
-    return project(tp, arrived, mine, partner)
+    same_core = [list(range(core, n_tp, 2)) for core in range(2)]
+    partner = across(w_out, swap)
+    keep, give = attend(
+        sp, lax.rem(tp, 2), query, own, (one, two, three, four, five, six), out_gain.reshape(1, -1), n_tp // 2
+    )
+    got = across(give, swap)
+    tiles = product(keep, got, w_out, partner)
+    arrived = lax.all_to_all(tiles, "tp", split_axis=0, concat_axis=0, axis_index_groups=same_core, tiled=True)
+    return finish(arrived, w_out.shape[1], n_tp * w_out.shape[0])
 
 
 def solution(mesh):

time: 107 us -> 81.2 us (0.76)
  the two profiles are of different devices: /device:TPU:744 before, /device:TPU:296 now
where the time goes in v2:
time: 81.2 us; the launch traced here: 80.8 us
  starting transfers between devices  48.6 us (60%)
  blocking collectives  17.6 us (22%)
  waiting for transfers between devices  7.55 us (9%)
  Pallas kernels  6.99 us (9%)
    ppermute x6, starting transfers between devices, ahead(): lax.ppermute(value, 'sp', [(source, source + steps) for source in range(f...  44.7 us
    all_to_all x1, blocking collectives, layer(): lax.all_to_all(tiles, 'tp', split_axis=0, concat_axis=0, axis_index_group...  17.6 us
    ppermute x6, waiting for transfers between devices, ahead(): lax.ppermute(value, 'sp', [(source, source + steps) for source in range(f...  6.29 us
    ppermute x2, starting transfers between devices, across(): return lax.ppermute(value, 'tp', pairs)  3.9 us
    pallas_call x1, Pallas kernels, qkv(): pl.pallas_call(functools.partial(qkv_kernel, chunks), out_shape=(jax.Shap...  3.23 us
    pallas_call x1, Pallas kernels, attend(): pl.pallas_call(attend_kernel, out_shape=(jax.ShapeDtypeStruct((parts, CLA...  2.36 us
  transfers between devices with their start and end apart: 8, of which 3 were waited for; matrix products, arithmetic and copies ran while one was open for 0% of the time, Pallas kernels for 3%

profile of v2, /device:TPU:296, one launch (start us, length us, event | category | flops | bytes accessed | tf_op | source)
XLA Modules:
  0.0 80.8 jit_solution(17230350804497731536)
XLA Ops:
  0.0 0.0 copy-start
  0.0 0.0 copy-start.1
  0.0 3.2 %qkv.1 = (bf16[4,96,128]{2,1,0:T(8,128)(2,1)S(1)}, bf16[4,96,256]{2,1,0:T(8,128)(2,1)S(1)}) custom-call(bf16[384,2048]{1,0:T(8,128)(2,1)} %tok_hbm.1, f32[1,2048]{1,0:T(1,128)} %bitcast.5, bf16[2048,128]{1,0:T(8,128)(2,1)} %wq_hbm.1, bf16[2048,128]{1,0:T(8,128)(2,1)} %wk_hbm.1, bf16[2048,128]{1,0:T(8,128)(2,1)} %wv_hbm.1), custom_call_target="tpu_custom_call" | custom-call | tf_op jit(solution)/shard_map/qkv/pallas_call | solution.py:82
  3.2 4.7 %collective-permute-start = (bf16[4,96,256]{2,1,0:T(8,128)(2,1)S(1)}, bf16[4,96,256]{2,1,0:T(8,128)(2,1)S(1)}, u32[]{:S(2)}, u32[]{:S(2)}) collective-permute-start(bf16[4,96,256]{2,1,0:T(8,128)(2,1)S(1)} %get-tuple-element.10.own), channel_id=1, source_target_pairs={{0,8},{8,16},{16,24},{24,32},{32,40},{40,48},{48,56},{56,64},{64,7... | collective-permute-start | bytes 589832 | tf_op jit(solution)/shard_map/ppermute | solution.py:266
  8.0 6.9 %collective-permute-start.1 = (bf16[4,96,256]{2,1,0:T(8,128)(2,1)S(1)}, bf16[4,96,256]{2,1,0:T(8,128)(2,1)S(1)}, u32[]{:S(2)}, u32[]{:S(2)}) collective-permute-start(bf16[4,96,256]{2,1,0:T(8,128)(2,1)S(1)} %get-tuple-element.10.own), channel_id=1, source_target_pairs={{0,16},{8,24},{16,32},{24,40},{32,48},{40,56},{48,64},{56,72},{64,... | collective-permute-start | bytes 589832 | tf_op jit(solution)/shard_map/ppermute | solution.py:266
  14.9 0.0 copy-done
  14.9 2.0 %collective-permute-start.7 = (bf16[128,2048]{1,0:T(8,128)(2,1)S(1)}, bf16[128,2048]{1,0:T(8,128)(2,1)S(1)}, u32[]{:S(2)}, u32[]{:S(2)}) collective-permute-start(bf16[128,2048]{1,0:T(8,128)(2,1)S(1)} %copy-done), channel_id=1, source_target_pairs={{0,1},{1,0},{2,3},{3,2},{4,5},{5,4},{6,7},{7,6},{8,9},{9,8},{10,11... | collective-permute-start | bytes 1572872 | tf_op jit(solution)/shard_map/ppermute | solution.py:270
  16.9 0.0 collective-permute-done.rest_0_
  16.9 8.1 %collective-permute-start.2 = (bf16[4,96,256]{2,1,0:T(8,128)(2,1)S(1)}, bf16[4,96,256]{2,1,0:T(8,128)(2,1)S(1)}, u32[]{:S(2)}, u32[]{:S(2)}) collective-permute-start(bf16[4,96,256]{2,1,0:T(8,128)(2,1)S(1)} %collective-permute-done.rest_0_), channel_id=1, source_target_pairs={{8,24},{16,32},{24,40},{32,48},{40,56},{48,64},{56,72},{64,80},{72... | collective-permute-start | bytes 589832 | tf_op jit(solution)/shard_map/ppermute | solution.py:266
  25.0 0.0 collective-permute-done.1.rest_1_
  25.0 6.9 %collective-permute-start.3 = (bf16[4,96,256]{2,1,0:T(8,128)(2,1)S(1)}, bf16[4,96,256]{2,1,0:T(8,128)(2,1)S(1)}, u32[]{:S(2)}, u32[]{:S(2)}) collective-permute-start(bf16[4,96,256]{2,1,0:T(8,128)(2,1)S(1)} %collective-permute-done.1.rest_1_), channel_id=1, source_target_pairs={{16,32},{24,40},{32,48},{40,56},{48,64},{56,72},{64,80},{72,88},{8... | collective-permute-start | bytes 589832 | tf_op jit(solution)/shard_map/ppermute | solution.py:266
  32.0 0.0 collective-permute-done.2.rest_2_
  32.0 8.2 %collective-permute-start.4 = (bf16[4,96,256]{2,1,0:T(8,128)(2,1)S(1)}, bf16[4,96,256]{2,1,0:T(8,128)(2,1)S(1)}, u32[]{:S(2)}, u32[]{:S(2)}) collective-permute-start(bf16[4,96,256]{2,1,0:T(8,128)(2,1)S(1)} %collective-permute-done.2.rest_2_), channel_id=1, source_target_pairs={{24,40},{32,48},{40,56},{48,64},{56,72},{64,80},{72,88},{80,96},{8... | collective-permute-start | bytes 589832 | tf_op jit(solution)/shard_map/ppermute | solution.py:266
  40.2 4.4 %collective-permute-done.3.rest_3_ = bf16[4,96,256]{2,1,0:T(8,128)(2,1)S(1)} collective-permute-done((bf16[4,96,256]{2,1,0:T(8,128)(2,1)S(1)}, bf16[4,96,256]{2,1,0:T(8,128)(2,1)S(1)}, u32[]{:S(2)}, u32[]{:S(2)}) %collective-permute-start.3) | collective-permute-done | bytes 196640 | tf_op jit(solution)/shard_map/ppermute | solution.py:266
  44.6 9.8 %collective-permute-start.5 = (bf16[4,32,256]{2,1,0:T(8,128)(2,1)S(1)}, bf16[4,32,256]{2,1,0:T(8,128)(2,1)S(1)}, u32[]{:S(2)}, u32[]{:S(2)}) collective-permute-start(bf16[4,32,256]{2,1,0:T(8,128)(2,1)S(1)} %slice.4), channel_id=1, source_target_pairs={{32,48},{40,56},{48,64},{56,72},{64,80},{72,88},{80,96},{88,104},{... | collective-permute-start | bytes 196616 | tf_op jit(solution)/shard_map/ppermute | solution.py:266
  54.4 1.9 %collective-permute-done.5.rest_5_ = bf16[4,32,256]{2,1,0:T(8,128)(2,1)S(1)} collective-permute-done((bf16[4,32,256]{2,1,0:T(8,128)(2,1)S(1)}, bf16[4,32,256]{2,1,0:T(8,128)(2,1)S(1)}, u32[]{:S(2)}, u32[]{:S(2)}) %collective-permute-start.5) | collective-permute-done | bytes 65568 | tf_op jit(solution)/shard_map/ppermute | solution.py:266
  56.3 0.0 collective-permute-done.4.rest_4_
  56.3 0.0 copy-done.1
  56.3 2.4 %attend.1 = (bf16[4,48,256]{2,1,0:T(8,128)(2,1)S(1)}, bf16[4,48,256]{2,1,0:T(8,128)(2,1)S(1)}) custom-call(s32[1]{0:T(128)} %bitcast.sp_ref, s32[1]{0:T(128)S(6)} %rem.18.core_ref, bf16[4,96,128]{2,1,0:T(8,128)(2,1)S(1)} %get-tuple-element.9.q_ref, bf16[4,96,256]{2,1,0:T(8,128)(2,1)S(1)} %get-tuple-element.10.own, ...), custom_call_target="tpu_custom_call" | custom-call | tf_op jit(solution)/shard_map/attend/pallas_call | solution.py:199
  58.6 2.0 %collective-permute-start.6 = (bf16[4,48,256]{2,1,0:T(8,128)(2,1)S(1)}, bf16[4,48,256]{2,1,0:T(8,128)(2,1)S(1)}, u32[]{:S(2)}, u32[]{:S(2)}) collective-permute-start(bf16[4,48,256]{2,1,0:T(8,128)(2,1)S(1)} %get-tuple-element.12), channel_id=1, source_target_pairs={{0,1},{1,0},{2,3},{3,2},{4,5},{5,4},{6,7},{7,6},{8,9},{9,8},{10,11... | collective-permute-start | bytes 294920 | tf_op jit(solution)/shard_map/ppermute | solution.py:270
  60.6 0.0 collective-permute-done.7.partner
  60.6 1.3 %collective-permute-done.6.got_ref = bf16[4,48,256]{2,1,0:T(8,128)(2,1)S(1)} collective-permute-done((bf16[4,48,256]{2,1,0:T(8,128)(2,1)S(1)}, bf16[4,48,256]{2,1,0:T(8,128)(2,1)S(1)}, u32[]{:S(2)}, u32[]{:S(2)}) %collective-permute-start.6) | collective-permute-done | bytes 98336 | tf_op jit(solution)/shard_map/ppermute | solution.py:270
  61.9 0.5 product.1
  62.4 17.6 %all_to_all.5.parts_ref = bf16[4,48,2176]{2,1,0:T(8,128)(2,1)S(1)} all-to-all(bf16[4,48,2176]{2,1,0:T(8,128)(2,1)S(1)} %product.1), channel_id=1, replica_groups={{0,2,4,6},{1,3,5,7},{8,10,12,14},{9,11,13,15},{16,18,20,22},{17,19,21,2..., dimensions={0} | all-to-all | bytes 1671168 | tf_op jit(solution)/shard_map/all_to_all | solution.py:296
  80.0 0.9 %finish.1 = bf16[48,2048]{1,0:T(8,128)(2,1)} custom-call(bf16[4,48,2176]{2,1,0:T(8,128)(2,1)S(1)} %all_to_all.5.parts_ref), custom_call_target="tpu_custom_call" | custom-call | tf_op jit(solution)/shard_map/finish/pallas_call | solution.py:254
  (1 shorter events, 0.0 us)
Async XLA Ops:
  0.0 14.9 %copy-start = (bf16[128,2048]{1,0:T(8,128)(2,1)S(1)}, bf16[128,2048]{1,0:T(8,128)(2,1)}, u32[]{:S(2)}) copy-start(bf16[128,2048]{1,0:T(8,128)(2,1)} %mine.1) | copy-start | bytes 1572868
  0.0 56.3 %copy-start.1 = (f32[128]{0:T(128)S(1)}, f32[128]{0:T(128)}, u32[]{:S(2)}) copy-start(f32[128]{0:T(128)} %param.12) | copy-start | bytes 1540
  3.2 13.6 %collective-permute-start = (bf16[4,96,256]{2,1,0:T(8,128)(2,1)S(1)}, bf16[4,96,256]{2,1,0:T(8,128)(2,1)S(1)}, u32[]{:S(2)}, u32[]{:S(2)}) collective-permute-start(bf16[4,96,256]{2,1,0:T(8,128)(2,1)S(1)} %get-tuple-element.10.own), channel_id=1, source_target_pairs={{0,8},{8,16},{16,24},{24,32},{32,40},{40,48},{48,56},{56,64},{64,7... | collective-permute-start | bytes 589832 | tf_op jit(solution)/shard_map/ppermute | solution.py:266
  8.0 17.1 %collective-permute-start.1 = (bf16[4,96,256]{2,1,0:T(8,128)(2,1)S(1)}, bf16[4,96,256]{2,1,0:T(8,128)(2,1)S(1)}, u32[]{:S(2)}, u32[]{:S(2)}) collective-permute-start(bf16[4,96,256]{2,1,0:T(8,128)(2,1)S(1)} %get-tuple-element.10.own), channel_id=1, source_target_pairs={{0,16},{8,24},{16,32},{24,40},{32,48},{40,56},{48,64},{56,72},{64,... | collective-permute-start | bytes 589832 | tf_op jit(solution)/shard_map/ppermute | solution.py:266
  14.9 45.7 %collective-permute-start.7 = (bf16[128,2048]{1,0:T(8,128)(2,1)S(1)}, bf16[128,2048]{1,0:T(8,128)(2,1)S(1)}, u32[]{:S(2)}, u32[]{:S(2)}) collective-permute-start(bf16[128,2048]{1,0:T(8,128)(2,1)S(1)} %copy-done), channel_id=1, source_target_pairs={{0,1},{1,0},{2,3},{3,2},{4,5},{5,4},{6,7},{7,6},{8,9},{9,8},{10,11... | collective-permute-start | bytes 1572872 | tf_op jit(solution)/shard_map/ppermute | solution.py:270
  16.9 15.1 %collective-permute-start.2 = (bf16[4,96,256]{2,1,0:T(8,128)(2,1)S(1)}, bf16[4,96,256]{2,1,0:T(8,128)(2,1)S(1)}, u32[]{:S(2)}, u32[]{:S(2)}) collective-permute-start(bf16[4,96,256]{2,1,0:T(8,128)(2,1)S(1)} %collective-permute-done.rest_0_), channel_id=1, source_target_pairs={{8,24},{16,32},{24,40},{32,48},{40,56},{48,64},{56,72},{64,80},{72... | collective-permute-start | bytes 589832 | tf_op jit(solution)/shard_map/ppermute | solution.py:266
  25.0 19.5 %collective-permute-start.3 = (bf16[4,96,256]{2,1,0:T(8,128)(2,1)S(1)}, bf16[4,96,256]{2,1,0:T(8,128)(2,1)S(1)}, u32[]{:S(2)}, u32[]{:S(2)}) collective-permute-start(bf16[4,96,256]{2,1,0:T(8,128)(2,1)S(1)} %collective-permute-done.1.rest_1_), channel_id=1, source_target_pairs={{16,32},{24,40},{32,48},{40,56},{48,64},{56,72},{64,80},{72,88},{8... | collective-permute-start | bytes 589832 | tf_op jit(solution)/shard_map/ppermute | solution.py:266
  32.0 24.3 %collective-permute-start.4 = (bf16[4,96,256]{2,1,0:T(8,128)(2,1)S(1)}, bf16[4,96,256]{2,1,0:T(8,128)(2,1)S(1)}, u32[]{:S(2)}, u32[]{:S(2)}) collective-permute-start(bf16[4,96,256]{2,1,0:T(8,128)(2,1)S(1)} %collective-permute-done.2.rest_2_), channel_id=1, source_target_pairs={{24,40},{32,48},{40,56},{48,64},{56,72},{64,80},{72,88},{80,96},{8... | collective-permute-start | bytes 589832 | tf_op jit(solution)/shard_map/ppermute | solution.py:266
  44.6 11.7 %collective-permute-start.5 = (bf16[4,32,256]{2,1,0:T(8,128)(2,1)S(1)}, bf16[4,32,256]{2,1,0:T(8,128)(2,1)S(1)}, u32[]{:S(2)}, u32[]{:S(2)}) collective-permute-start(bf16[4,32,256]{2,1,0:T(8,128)(2,1)S(1)} %slice.4), channel_id=1, source_target_pairs={{32,48},{40,56},{48,64},{56,72},{64,80},{72,88},{80,96},{88,104},{... | collective-permute-start | bytes 196616 | tf_op jit(solution)/shard_map/ppermute | solution.py:266
  58.6 3.2 %collective-permute-start.6 = (bf16[4,48,256]{2,1,0:T(8,128)(2,1)S(1)}, bf16[4,48,256]{2,1,0:T(8,128)(2,1)S(1)}, u32[]{:S(2)}, u32[]{:S(2)}) collective-permute-start(bf16[4,48,256]{2,1,0:T(8,128)(2,1)S(1)} %get-tuple-element.12), channel_id=1, source_target_pairs={{0,1},{1,0},{2,3},{3,2},{4,5},{5,4},{6,7},{7,6},{8,9},{9,8},{10,11... | collective-permute-start | bytes 294920 | tf_op jit(solution)/shard_map/ppermute | solution.py:270

commit v3 on v2

--- a/solution.py
+++ b/solution.py
@@ -115,72 +115,121 @@
     return spread.astype(BF16)
 
 
-def attend_kernel(sp_ref, core_ref, q_ref, own, *rest):
-    older = rest[:-6]
-    gain_ref, keep_ref, give_ref, k_all, v_all, natural = rest[-6:]
-    width = q_ref.shape[2]
-    share = q_ref.shape[1]
-    far = WINDOW_THIRD // CLASSES
+def both_heads(query, lane):
+    zero = jnp.zeros_like(query)
+    return jnp.concatenate([jnp.where(lane < HEAD_DIM, query, zero), jnp.where(lane < HEAD_DIM, zero, query)], axis=0)
+
+
+def twice(value):
+    return jnp.concatenate([value, value], axis=0)
+
+
+def third_hit(lag):
+    ratio = DILATION_THIRD // CLASSES
+    reach = WINDOW_THIRD // CLASSES
+    return jnp.logical_and(lag <= reach, lax.rem(lag, ratio) == 0)
+
+
+CONTRACT = (((1,), (1,)), ((), ()))
+
+
+def near_kernel(sp_ref, q_ref, own, *rest):
+    older = rest[:-5]
+    top_ref, norm_ref, sum_ref, k_all, v_all = rest[-5:]
+    share, width = q_ref.shape[1:]
+    span = k_all.shape[1]
+    far = span - share
     near = WINDOW_FIRST // CLASSES
-    span = far + share
     tail = near + share
     start = span
     for block in (own, *older):
-        count = block.shape[1]
-        start -= count
+        start -= share
         for c in range(CLASSES):
-            k_all[c, start : start + count, :] = block[c, :, 0:width]
-            v_all[c, start : start + count, :] = block[c, :, width : 2 * width]
+            k_all[c, start : start + share, :] = block[c, :, 0:width]
+            v_all[c, start : start + share, :] = block[c, :, width : 2 * width]
     sp = sp_ref[0]
     row = lax.broadcasted_iota(jnp.int32, (share, span), 0)
     col = lax.broadcasted_iota(jnp.int32, (share, span), 1)
     lag = row - col + far
-    ratio = DILATION_THIRD // CLASSES
-    behind = (lag >= 0).astype(F32)
-    count = behind * (
+    behind = lag >= 0
+    lag = jnp.maximum(lag, 0)
+    count = (
         (lag <= WINDOW_FIRST // CLASSES).astype(F32)
         + (lag <= WINDOW_SECOND // CLASSES).astype(F32)
-        + jnp.logical_and(lag <= far, lax.rem(lag + ratio * span, ratio) == 0).astype(F32)
+        + third_hit(lag).astype(F32)
     )
-    live = jnp.logical_and(count > 0.5, col >= far - share * sp)
+    live = jnp.logical_and(jnp.logical_and(behind, count > 0.5), col >= far - share * sp)
     weight = jnp.where(count > 2.5, jnp.log(F32(3.0)), jnp.where(count > 1.5, jnp.log(F32(2.0)), F32(0.0)))
-    bias = jnp.where(live, weight, NEG)
-    bias = jnp.concatenate([bias, bias], axis=0)
+    bias = twice(jnp.where(live, weight, NEG))
     row = lax.broadcasted_iota(jnp.int32, (share, tail), 0)
     col = lax.broadcasted_iota(jnp.int32, (share, tail), 1)
     lag = row - col + near
     there = col >= near - share * sp
-    after = jnp.where(jnp.logical_and(there, jnp.logical_and(lag >= 0, lag < near)), F32(0.0), NEG)
-    before = jnp.where(jnp.logical_and(there, jnp.logical_and(lag >= 1, lag <= near)), F32(0.0), NEG)
-    after = jnp.concatenate([after, after], axis=0)
-    before = jnp.concatenate([before, before], axis=0)
+    after = twice(jnp.where(jnp.logical_and(there, jnp.logical_and(lag >= 0, lag < near)), F32(0.0), NEG))
+    before = twice(jnp.where(jnp.logical_and(there, jnp.logical_and(lag >= 1, lag <= near)), F32(0.0), NEG))
     lane = lax.broadcasted_iota(jnp.int32, (share, width), 1)
-    contract = (((1,), (1,)), ((), ()))
     for c in range(CLASSES):
-        query = q_ref[c]
-        zero = jnp.zeros_like(query)
-        stacked = jnp.concatenate(
-            [jnp.where(lane < HEAD_DIM, query, zero), jnp.where(lane < HEAD_DIM, zero, query)], axis=0
-        )
-        scores = [lax.dot_general(stacked, k_all[c], contract, preferred_element_type=F32) + bias]
+        stacked = both_heads(q_ref[c], lane)
+        scores = [lax.dot_general(stacked, k_all[c], CONTRACT, preferred_element_type=F32) + bias]
         values = [v_all[c]]
         for other in range(CLASSES):
             if other != c:
                 part = lax.dot_general(
-                    stacked, k_all[other, span - tail : span, :], contract, preferred_element_type=F32
+                    stacked, k_all[other, span - tail : span, :], CONTRACT, preferred_element_type=F32
                 )
                 scores.append(part + (after if c > other else before))
                 values.append(v_all[other, span - tail : span, :])
         top = functools.reduce(jnp.maximum, [jnp.max(part, axis=-1, keepdims=True) for part in scores])
         weights = [jnp.exp(part - top) for part in scores]
-        norm = functools.reduce(jnp.add, [jnp.sum(part, axis=-1, keepdims=True) for part in weights])
-        mixed = functools.reduce(
+        top_ref[c] = top
+        norm_ref[c] = functools.reduce(jnp.add, [jnp.sum(part, axis=-1, keepdims=True) for part in weights])
+        sum_ref[c] = functools.reduce(
             jnp.add,
             [
                 jnp.dot(part.astype(BF16), value, preferred_element_type=F32)
                 for part, value in zip(weights, values)
             ],
         )
+
+
+def attend_near(sp, query, own, older):
+    share, width = query.shape[1:]
+    span = (1 + len(older)) * share
+    return pl.pallas_call(
+        near_kernel,
+        out_shape=(
+            jax.ShapeDtypeStruct((CLASSES, 2 * share, 1), F32),
+            jax.ShapeDtypeStruct((CLASSES, 2 * share, 1), F32),
+            jax.ShapeDtypeStruct((CLASSES, 2 * share, width), F32),
+        ),
+        in_specs=[pl.BlockSpec(memory_space=pltpu.SMEM)]
+        + [pl.BlockSpec(memory_space=VMEM)] * (2 + len(older)),
+        out_specs=(pl.BlockSpec(memory_space=VMEM),) * 3,
+        scratch_shapes=[VMEM((CLASSES, span, width), BF16), VMEM((CLASSES, span, width), BF16)],
+        compiler_params=pltpu.CompilerParams(vmem_limit_bytes=20 << 20),
+        name="attend_near",
+    )(sp, query, own, *older)
+
+
+def far_kernel(sp_ref, core_ref, q_ref, five, six, top_ref, norm_ref, sum_ref, gain_ref, keep_ref, give_ref, natural):
+    share, width = q_ref.shape[1:]
+    count = five.shape[1] + six.shape[1]
+    far = WINDOW_THIRD // CLASSES
+    row = lax.broadcasted_iota(jnp.int32, (share, count), 0)
+    col = lax.broadcasted_iota(jnp.int32, (share, count), 1)
+    live = jnp.logical_and(third_hit(row - col + far), col >= far - share * sp_ref[0])
+    bias = twice(jnp.where(live, F32(0.0), NEG))
+    lane = lax.broadcasted_iota(jnp.int32, (share, width), 1)
+    for c in range(CLASSES):
+        stacked = both_heads(q_ref[c], lane)
+        keys = jnp.concatenate([six[c, :, 0:width], five[c, :, 0:width]], axis=0)
+        values = jnp.concatenate([six[c, :, width : 2 * width], five[c, :, width : 2 * width]], axis=0)
+        score = lax.dot_general(stacked, keys, CONTRACT, preferred_element_type=F32) + bias
+        top = jnp.maximum(top_ref[c], jnp.max(score, axis=-1, keepdims=True))
+        shrink = jnp.exp(top_ref[c] - top)
+        weight = jnp.exp(score - top)
+        norm = norm_ref[c] * shrink + jnp.sum(weight, axis=-1, keepdims=True)
+        mixed = sum_ref[c] * shrink + jnp.dot(weight.astype(BF16), values, preferred_element_type=F32)
         mixed = mixed / norm
         natural[pl.ds(c, share, stride=CLASSES), :] = jnp.where(lane < HEAD_DIM, mixed[:share], mixed[share:])
     core = core_ref[0]
@@ -193,23 +242,17 @@
             target[place, :, width : 2 * width] = split(jnp.sum(block * block, axis=-1, keepdims=True), width)
 
 
-def attend(sp, core, query, own, older, gain, parts):
+def attend_far(sp, core, query, five, six, state, gain, parts):
     share, width = query.shape[1:]
-    span = WINDOW_THIRD // CLASSES + share
-    return pl.pallas_call(
-        attend_kernel,
+    return pl.pallas_call(
+        far_kernel,
         out_shape=(jax.ShapeDtypeStruct((parts, CLASSES * share // (2 * parts), 2 * width), BF16),) * 2,
-        in_specs=[pl.BlockSpec(memory_space=pltpu.SMEM)] * 2
-        + [pl.BlockSpec(memory_space=VMEM)] * (3 + len(older)),
+        in_specs=[pl.BlockSpec(memory_space=pltpu.SMEM)] * 2 + [pl.BlockSpec(memory_space=VMEM)] * 7,
         out_specs=(pl.BlockSpec(memory_space=VMEM),) * 2,
-        scratch_shapes=[
-            VMEM((CLASSES, span, width), BF16),
-            VMEM((CLASSES, span, width), BF16),
-            VMEM((CLASSES * share, width), F32),
-        ],
-        compiler_params=pltpu.CompilerParams(vmem_limit_bytes=20 << 20),
-        name="attend",
-    )(sp, core, query, own, *older, gain)
+        scratch_shapes=[VMEM((CLASSES * share, width), F32)],
+        compiler_params=pltpu.CompilerParams(vmem_limit_bytes=20 << 20),
+        name="attend_far",
+    )(sp, core, query, five, six, *state, gain)
 
 
 def product_kernel(keep_ref, got_ref, mine, partner, out_ref):
@@ -279,18 +322,17 @@
 
     one = ahead(own, 1, 0)
     two = ahead(own, 2, 0)
-    three = ahead(one, 2, 1)
+    three = ahead(two, 1, 2)
     four = ahead(two, 2, 2)
-    five = ahead(three, 2, 3)
+    five = ahead(four, 1, 4)
     excess = 6 * (tok_rows // CLASSES) - WINDOW_THIRD // CLASSES
     six = ahead(four[:, excess:, :], 2, 4)
 
     swap = [(n, n ^ 1) for n in range(n_tp)]
     same_core = [list(range(core, n_tp, 2)) for core in range(2)]
     partner = across(w_out, swap)
-    keep, give = attend(
-        sp, lax.rem(tp, 2), query, own, (one, two, three, four, five, six), out_gain.reshape(1, -1), n_tp // 2
-    )
+    state = attend_near(sp, query, own, (one, two, three, four))
+    keep, give = attend_far(sp, lax.rem(tp, 2), query, five, six, state, out_gain.reshape(1, -1), n_tp // 2)
     got = across(give, swap)
     tiles = product(keep, got, w_out, partner)
     arrived = lax.all_to_all(tiles, "tp", split_axis=0, concat_axis=0, axis_index_groups=same_core, tiled=True)

time: 81.2 us -> 79.5 us (0.979)
  the two profiles are of different devices: /device:TPU:296 before, /device:TPU:96 now
where the time goes in v3:
time: 79.5 us; the launch traced here: 79.1 us
  starting transfers between devices  49.3 us (62%)
  blocking collectives  15.8 us (20%)
  Pallas kernels  7.91 us (10%)
  waiting for transfers between devices  5.9 us (7%)
    ppermute x6, starting transfers between devices, ahead(): lax.ppermute(value, 'sp', [(source, source + steps) for source in range(f...  45.4 us
    all_to_all x1, blocking collectives, layer(): lax.all_to_all(tiles, 'tp', split_axis=0, concat_axis=0, axis_index_group...  15.8 us
    ppermute x6, waiting for transfers between devices, ahead(): lax.ppermute(value, 'sp', [(source, source + steps) for source in range(f...  4.64 us
    ppermute x2, starting transfers between devices, across(): return lax.ppermute(value, 'tp', pairs)  3.9 us
    pallas_call x1, Pallas kernels, qkv(): pl.pallas_call(functools.partial(qkv_kernel, chunks), out_shape=(jax.Shap...  3.23 us
    pallas_call x1, Pallas kernels, attend_near(): pl.pallas_call(near_kernel, out_shape=(jax.ShapeDtypeStruct((CLASSES, 2 *...  1.97 us
  transfers between devices with their start and end apart: 8, of which 3 were waited for; matrix products, arithmetic and copies ran while one was open for 0% of the time, Pallas kernels for 4%

profile of v3, /device:TPU:96, one launch (start us, length us, event | category | flops | bytes accessed | tf_op | source)
XLA Modules:
  0.0 79.1 jit_solution(2124846888030186642)
XLA Ops:
  0.0 0.0 copy-start
  0.0 0.0 copy-start.1
  0.0 3.2 %qkv.1 = (bf16[4,96,128]{2,1,0:T(8,128)(2,1)S(1)}, bf16[4,96,256]{2,1,0:T(8,128)(2,1)S(1)}) custom-call(bf16[384,2048]{1,0:T(8,128)(2,1)} %tok_hbm.1, f32[1,2048]{1,0:T(1,128)} %bitcast.5, bf16[2048,128]{1,0:T(8,128)(2,1)} %wq_hbm.1, bf16[2048,128]{1,0:T(8,128)(2,1)} %wk_hbm.1, bf16[2048,128]{1,0:T(8,128)(2,1)} %wv_hbm.1), custom_call_target="tpu_custom_call" | custom-call | tf_op jit(solution)/shard_map/qkv/pallas_call | solution.py:82
  3.2 6.9 %collective-permute-start = (bf16[4,96,256]{2,1,0:T(8,128)(2,1)S(1)}, bf16[4,96,256]{2,1,0:T(8,128)(2,1)S(1)}, u32[]{:S(2)}, u32[]{:S(2)}) collective-permute-start(bf16[4,96,256]{2,1,0:T(8,128)(2,1)S(1)} %get-tuple-element.13.own), channel_id=1, source_target_pairs={{0,16},{8,24},{16,32},{24,40},{32,48},{40,56},{48,64},{56,72},{64,... | collective-permute-start | bytes 589832 | tf_op jit(solution)/shard_map/ppermute | solution.py:309
  10.2 0.0 copy-done
  10.2 2.0 %collective-permute-start.7 = (bf16[128,2048]{1,0:T(8,128)(2,1)S(1)}, bf16[128,2048]{1,0:T(8,128)(2,1)S(1)}, u32[]{:S(2)}, u32[]{:S(2)}) collective-permute-start(bf16[128,2048]{1,0:T(8,128)(2,1)S(1)} %copy-done), channel_id=1, source_target_pairs={{0,1},{1,0},{2,3},{3,2},{4,5},{5,4},{6,7},{7,6},{8,9},{9,8},{10,11... | collective-permute-start | bytes 1572872 | tf_op jit(solution)/shard_map/ppermute | solution.py:313
  12.2 3.5 %collective-permute-done.rest_1_ = bf16[4,96,256]{2,1,0:T(8,128)(2,1)S(1)} collective-permute-done((bf16[4,96,256]{2,1,0:T(8,128)(2,1)S(1)}, bf16[4,96,256]{2,1,0:T(8,128)(2,1)S(1)}, u32[]{:S(2)}, u32[]{:S(2)}) %collective-permute-start) | collective-permute-done | bytes 196640 | tf_op jit(solution)/shard_map/ppermute | solution.py:309
  15.7 0.7 collective-permute-start.1
  16.4 35.8 %collective-permute-start.4 = (bf16[4,96,256]{2,1,0:T(8,128)(2,1)S(1)}, bf16[4,96,256]{2,1,0:T(8,128)(2,1)S(1)}, u32[]{:S(2)}, u32[]{:S(2)}) collective-permute-start(bf16[4,96,256]{2,1,0:T(8,128)(2,1)S(1)} %get-tuple-element.13.own), channel_id=1, source_target_pairs={{0,8},{8,16},{16,24},{24,32},{32,40},{40,48},{48,56},{56,64},{64,7... | collective-permute-start | bytes 589832 | tf_op jit(solution)/shard_map/ppermute | solution.py:309
  52.2 0.7 collective-permute-start.5
  52.8 0.0 collective-permute-done.1.rest_3_
  52.9 0.7 collective-permute-start.2
  53.5 0.7 collective-permute-start.3
  54.2 1.1 %collective-permute-done.4.rest_0_ = bf16[4,96,256]{2,1,0:T(8,128)(2,1)S(1)} collective-permute-done((bf16[4,96,256]{2,1,0:T(8,128)(2,1)S(1)}, bf16[4,96,256]{2,1,0:T(8,128)(2,1)S(1)}, u32[]{:S(2)}, u32[]{:S(2)}) %collective-permute-start.4) | collective-permute-done | bytes 196640 | tf_op jit(solution)/shard_map/ppermute | solution.py:309
  55.3 0.0 collective-permute-done.5.rest_2_
  55.3 2.0 %attend_near.1 = (f32[4,192,1]{2,1,0:T(8,128)S(1)}, f32[4,192,1]{2,1,0:T(8,128)S(1)}, f32[4,192,128]{2,1,0:T(8,128)S(1)}) custom-call(s32[1]{0:T(128)} %bitcast.sp_ref, bf16[4,96,128]{2,1,0:T(8,128)(2,1)S(1)} %get-tuple-element.12.q_ref, bf16[4,96,256]{2,1,0:T(8,128)(2,1)S(1)} %get-tuple-element.13.own, ...), custom_call_target="tpu_custom_call" | custom-call | tf_op jit(solution)/shard_map/attend_near/pallas_call | solution.py:198
  57.3 0.0 collective-permute-done.3.six
  57.3 0.0 collective-permute-done.2.five
  57.3 0.0 copy-done.1
  57.3 1.3 %attend_far.1 = (bf16[4,48,256]{2,1,0:T(8,128)(2,1)S(1)}, bf16[4,48,256]{2,1,0:T(8,128)(2,1)S(1)}) custom-call(s32[1]{0:T(128)} %bitcast.sp_ref, s32[1]{0:T(128)S(6)} %rem.18.core_ref, bf16[4,96,128]{2,1,0:T(8,128)(2,1)S(1)} %get-tuple-element.12.q_ref, bf16[4,96,256]{2,1,0:T(8,128)(2,1)S(1)} %collective-permute-done.2.five, ...), custom_call_target="tpu_custom_call" | custom-call | tf_op jit(solution)/shard_map/attend_far/pallas_call | solution.py:247
  58.7 2.0 %collective-permute-start.6 = (bf16[4,48,256]{2,1,0:T(8,128)(2,1)S(1)}, bf16[4,48,256]{2,1,0:T(8,128)(2,1)S(1)}, u32[]{:S(2)}, u32[]{:S(2)}) collective-permute-start(bf16[4,48,256]{2,1,0:T(8,128)(2,1)S(1)} %get-tuple-element.18), channel_id=1, source_target_pairs={{0,1},{1,0},{2,3},{3,2},{4,5},{5,4},{6,7},{7,6},{8,9},{9,8},{10,11... | collective-permute-start | bytes 294920 | tf_op jit(solution)/shard_map/ppermute | solution.py:313
  60.6 0.0 collective-permute-done.7.partner
  60.6 1.3 %collective-permute-done.6.got_ref = bf16[4,48,256]{2,1,0:T(8,128)(2,1)S(1)} collective-permute-done((bf16[4,48,256]{2,1,0:T(8,128)(2,1)S(1)}, bf16[4,48,256]{2,1,0:T(8,128)(2,1)S(1)}, u32[]{:S(2)}, u32[]{:S(2)}) %collective-permute-start.6) | collective-permute-done | bytes 98336 | tf_op jit(solution)/shard_map/ppermute | solution.py:313
  61.9 0.5 product.1
  62.4 15.8 %all_to_all.5.parts_ref = bf16[4,48,2176]{2,1,0:T(8,128)(2,1)S(1)} all-to-all(bf16[4,48,2176]{2,1,0:T(8,128)(2,1)S(1)} %product.1), channel_id=1, replica_groups={{0,2,4,6},{1,3,5,7},{8,10,12,14},{9,11,13,15},{16,18,20,22},{17,19,21,2..., dimensions={0} | all-to-all | bytes 1671168 | tf_op jit(solution)/shard_map/all_to_all | solution.py:338
  78.3 0.9 %finish.1 = bf16[48,2048]{1,0:T(8,128)(2,1)} custom-call(bf16[4,48,2176]{2,1,0:T(8,128)(2,1)S(1)} %all_to_all.5.parts_ref), custom_call_target="tpu_custom_call" | custom-call | tf_op jit(solution)/shard_map/finish/pallas_call | solution.py:297
  (1 shorter events, 0.0 us)
Async XLA Ops:
  0.0 10.2 %copy-start = (bf16[128,2048]{1,0:T(8,128)(2,1)S(1)}, bf16[128,2048]{1,0:T(8,128)(2,1)}, u32[]{:S(2)}) copy-start(bf16[128,2048]{1,0:T(8,128)(2,1)} %mine.1) | copy-start | bytes 1572868
  0.0 57.3 %copy-start.1 = (f32[128]{0:T(128)S(1)}, f32[128]{0:T(128)}, u32[]{:S(2)}) copy-start(f32[128]{0:T(128)} %param.12) | copy-start | bytes 1540
  3.2 12.4 %collective-permute-start = (bf16[4,96,256]{2,1,0:T(8,128)(2,1)S(1)}, bf16[4,96,256]{2,1,0:T(8,128)(2,1)S(1)}, u32[]{:S(2)}, u32[]{:S(2)}) collective-permute-start(bf16[4,96,256]{2,1,0:T(8,128)(2,1)S(1)} %get-tuple-element.13.own), channel_id=1, source_target_pairs={{0,16},{8,24},{16,32},{24,40},{32,48},{40,56},{48,64},{56,72},{64,... | collective-permute-start | bytes 589832 | tf_op jit(solution)/shard_map/ppermute | solution.py:309
  10.2 50.4 %collective-permute-start.7 = (bf16[128,2048]{1,0:T(8,128)(2,1)S(1)}, bf16[128,2048]{1,0:T(8,128)(2,1)S(1)}, u32[]{:S(2)}, u32[]{:S(2)}) collective-permute-start(bf16[128,2048]{1,0:T(8,128)(2,1)S(1)} %copy-done), channel_id=1, source_target_pairs={{0,1},{1,0},{2,3},{3,2},{4,5},{5,4},{6,7},{7,6},{8,9},{9,8},{10,11... | collective-permute-start | bytes 1572872 | tf_op jit(solution)/shard_map/ppermute | solution.py:313
  15.7 37.1 %collective-permute-start.1 = (bf16[4,96,256]{2,1,0:T(8,128)(2,1)S(1)}, bf16[4,96,256]{2,1,0:T(8,128)(2,1)S(1)}, u32[]{:S(2)}, u32[]{:S(2)}) collective-permute-start(bf16[4,96,256]{2,1,0:T(8,128)(2,1)S(1)} %collective-permute-done.rest_1_), channel_id=1, source_target_pairs={{16,32},{24,40},{32,48},{40,56},{48,64},{56,72},{64,80},{72,88},{8... | collective-permute-start | bytes 589832 | tf_op jit(solution)/shard_map/ppermute | solution.py:309
  16.4 39.0 %collective-permute-start.4 = (bf16[4,96,256]{2,1,0:T(8,128)(2,1)S(1)}, bf16[4,96,256]{2,1,0:T(8,128)(2,1)S(1)}, u32[]{:S(2)}, u32[]{:S(2)}) collective-permute-start(bf16[4,96,256]{2,1,0:T(8,128)(2,1)S(1)} %get-tuple-element.13.own), channel_id=1, source_target_pairs={{0,8},{8,16},{16,24},{24,32},{32,40},{40,48},{48,56},{56,64},{64,7... | collective-permute-start | bytes 589832 | tf_op jit(solution)/shard_map/ppermute | solution.py:309
  52.2 3.2 %collective-permute-start.5 = (bf16[4,96,256]{2,1,0:T(8,128)(2,1)S(1)}, bf16[4,96,256]{2,1,0:T(8,128)(2,1)S(1)}, u32[]{:S(2)}, u32[]{:S(2)}) collective-permute-start(bf16[4,96,256]{2,1,0:T(8,128)(2,1)S(1)} %collective-permute-done.rest_1_), channel_id=1, source_target_pairs={{16,24},{24,32},{32,40},{40,48},{48,56},{56,64},{64,72},{72,80},{8... | collective-permute-start | bytes 589832 | tf_op jit(solution)/shard_map/ppermute | solution.py:309
  52.9 4.5 %collective-permute-start.2 = (bf16[4,96,256]{2,1,0:T(8,128)(2,1)S(1)}, bf16[4,96,256]{2,1,0:T(8,128)(2,1)S(1)}, u32[]{:S(2)}, u32[]{:S(2)}) collective-permute-start(bf16[4,96,256]{2,1,0:T(8,128)(2,1)S(1)} %collective-permute-done.1.rest_3_), channel_id=1, source_target_pairs={{32,40},{40,48},{48,56},{56,64},{64,72},{72,80},{80,88},{88,96},{9... | collective-permute-start | bytes 589832 | tf_op jit(solution)/shard_map/ppermute | solution.py:309
  53.5 3.8 %collective-permute-start.3 = (bf16[4,32,256]{2,1,0:T(8,128)(2,1)S(1)}, bf16[4,32,256]{2,1,0:T(8,128)(2,1)S(1)}, u32[]{:S(2)}, u32[]{:S(2)}) collective-permute-start(bf16[4,32,256]{2,1,0:T(8,128)(2,1)S(1)} %slice.4), channel_id=1, source_target_pairs={{32,48},{40,56},{48,64},{56,72},{64,80},{72,88},{80,96},{88,104},{... | collective-permute-start | bytes 196616 | tf_op jit(solution)/shard_map/ppermute | solution.py:309
  58.7 3.2 %collective-permute-start.6 = (bf16[4,48,256]{2,1,0:T(8,128)(2,1)S(1)}, bf16[4,48,256]{2,1,0:T(8,128)(2,1)S(1)}, u32[]{:S(2)}, u32[]{:S(2)}) collective-permute-start(bf16[4,48,256]{2,1,0:T(8,128)(2,1)S(1)} %get-tuple-element.18), channel_id=1, source_target_pairs={{0,1},{1,0},{2,3},{3,2},{4,5},{5,4},{6,7},{7,6},{8,9},{9,8},{10,11... | collective-permute-start | bytes 294920 | tf_op jit(solution)/shard_map/ppermute | solution.py:313

commit v4 on v3

--- a/solution.py
+++ b/solution.py
@@ -15,6 +15,7 @@
 WINDOW_THIRD = 2048
 DILATION_THIRD = 16
 CLASSES = DILATION_SECOND
+EXTRA = 16
 
 EPS = 1e-06
 NEG = -1e30
@@ -48,7 +49,6 @@
         copies.append(pair)
     gain_copy.wait()
     squares = jnp.zeros((rows, 128), F32)
-    total = jnp.zeros((rows, 3 * width), F32)
     for n in range(chunks):
         for copy in copies[n]:
             copy.wait()
@@ -56,8 +56,8 @@
         for lane in range(0, piece, 128):
             part = block[:, lane : lane + 128]
             squares = squares + part * part
-        scaled = (block * gain_ref[:, n * piece : (n + 1) * piece]).astype(BF16)
-        total = total + jnp.dot(scaled, w[n * piece : (n + 1) * piece, :], preferred_element_type=F32)
+        tok[:, n * piece : (n + 1) * piece] = (block * gain_ref[:, n * piece : (n + 1) * piece]).astype(BF16)
+    total = jnp.dot(tok[...], w[...], preferred_element_type=F32)
     inverse = lax.rsqrt(jnp.sum(squares, axis=-1, keepdims=True) / depth + EPS)
     total = total * inverse
     for m in range(3):
@@ -77,7 +77,7 @@
 def qkv(tokens, norm_gain, w_query, w_key, w_value):
     rows, depth = tokens.shape
     width = w_query.shape[1]
-    chunks = 4
+    chunks = 2
     share = rows // CLASSES
     return pl.pallas_call(
         functools.partial(qkv_kernel, chunks),
@@ -255,6 +255,12 @@
     )(sp, core, query, five, six, *state, gain)
 
 
+def turned(column_or_row, rows, axis):
+    shape = (rows, 128)
+    same = lax.broadcasted_iota(jnp.int32, shape, 0) == lax.broadcasted_iota(jnp.int32, shape, 1)
+    return jnp.sum(jnp.where(same, column_or_row, F32(0.0)), axis=axis, keepdims=True)
+
+
 def product_kernel(keep_ref, got_ref, mine, partner, out_ref):
     parts, rows, double = keep_ref.shape
     width = double // 2
@@ -264,15 +270,25 @@
     total = jnp.dot(keep[:, :width], mine[...], preferred_element_type=F32)
     total = total + jnp.dot(got[:, :width], partner[...], preferred_element_type=F32)
     squares = jnp.sum(keep[:, width:].astype(F32) + got[:, width:].astype(F32), axis=-1, keepdims=True)
-    out_ref[:, :, 0:columns] = total.astype(BF16).reshape(parts, rows, columns)
-    out_ref[:, :, columns : columns + width] = split(squares, width).reshape(parts, rows, width)
+    below = rows * columns // 128
+    line = lax.broadcasted_iota(jnp.int32, (EXTRA, 128), 0)
+    for place in range(parts):
+        mine_rows = slice(place * rows, (place + 1) * rows)
+        for n in range(columns // 128):
+            out_ref[place, n * rows : (n + 1) * rows, :] = total[mine_rows, n * 128 : (n + 1) * 128].astype(BF16)
+        whole = turned(squares[mine_rows], rows, 0)
+        high = whole.astype(BF16).astype(F32)
+        middle = (whole - high).astype(BF16).astype(F32)
+        low = whole - high - middle
+        extra = jnp.where(line == 0, high, jnp.where(line == 1, middle, jnp.where(line == 2, low, F32(0.0))))
+        out_ref[place, below : below + EXTRA, :] = extra.astype(BF16)
 
 
 def product(keep, got, mine, partner):
-    parts, rows, double = keep.shape
+    parts, rows, _ = keep.shape
     return pl.pallas_call(
         product_kernel,
-        out_shape=jax.ShapeDtypeStruct((parts, rows, mine.shape[1] + double // 2), BF16),
+        out_shape=jax.ShapeDtypeStruct((parts, rows * mine.shape[1] // 128 + EXTRA, 128), BF16),
         in_specs=[pl.BlockSpec(memory_space=VMEM)] * 4,
         out_specs=pl.BlockSpec(memory_space=VMEM),
         compiler_params=pltpu.CompilerParams(vmem_limit_bytes=20 << 20),
@@ -281,22 +297,25 @@
 
 
 def finish_kernel(channels, parts_ref, out_ref):
-    parts, rows, columns = parts_ref.shape
-    wide = out_ref.shape[1]
-    squares = jnp.zeros((rows, columns - wide), F32)
-    for n in range(parts):
-        squares = squares + parts_ref[n, :, wide:columns].astype(F32)
-    scale = lax.rsqrt(jnp.sum(squares, axis=-1, keepdims=True) / channels + EPS)
-    total = parts_ref[0, :, 0:wide].astype(F32)
-    for n in range(1, parts):
-        total = total + parts_ref[n, :, 0:wide].astype(F32)
-    out_ref[...] = (total * scale).astype(BF16)
-
-
-def finish(arrived, wide, channels):
+    parts = parts_ref.shape[0]
+    rows, columns = out_ref.shape
+    below = rows * columns // 128
+    squares = functools.reduce(
+        jnp.add, [parts_ref[place, below : below + EXTRA, :].astype(F32) for place in range(parts)]
+    )
+    squares = turned(jnp.sum(squares, axis=0, keepdims=True), rows, 1)
+    scale = lax.rsqrt(squares / channels + EPS)
+    for n in range(columns // 128):
+        total = functools.reduce(
+            jnp.add, [parts_ref[place, n * rows : (n + 1) * rows, :].astype(F32) for place in range(parts)]
+        )
+        out_ref[:, n * 128 : (n + 1) * 128] = (total * scale).astype(BF16)
+
+
+def finish(arrived, rows, wide, channels):
     return pl.pallas_call(
         functools.partial(finish_kernel, channels),
-        out_shape=jax.ShapeDtypeStruct((arrived.shape[1], wide), BF16),
+        out_shape=jax.ShapeDtypeStruct((rows, wide), BF16),
         in_specs=[pl.BlockSpec(memory_space=VMEM)],
         out_specs=pl.BlockSpec(memory_space=VMEM),
         compiler_params=pltpu.CompilerParams(vmem_limit_bytes=20 << 20),
@@ -336,7 +355,7 @@
     got = across(give, swap)
     tiles = product(keep, got, w_out, partner)
     arrived = lax.all_to_all(tiles, "tp", split_axis=0, concat_axis=0, axis_index_groups=same_core, tiled=True)
-    return finish(arrived, w_out.shape[1], n_tp * w_out.shape[0])
+    return finish(arrived, tok_rows // n_tp, w_out.shape[1], n_tp * w_out.shape[0])
 
 
 def solution(mesh):

time: 79.5 us -> 78.8 us (level)
  no operation moved by 1% of the time
where the time goes in v4:
time: 78.8 us; the launch traced here: 78.5 us
  starting transfers between devices  49.3 us (63%)
  blocking collectives  15.5 us (20%)
  Pallas kernels  7.62 us (10%)
  waiting for transfers between devices  5.91 us (8%)
    ppermute x6, starting transfers between devices, ahead(): lax.ppermute(value, 'sp', [(source, source + steps) for source in range(f...  45.4 us
    all_to_all x1, blocking collectives, layer(): lax.all_to_all(tiles, 'tp', split_axis=0, concat_axis=0, axis_index_group...  15.5 us
    ppermute x6, waiting for transfers between devices, ahead(): lax.ppermute(value, 'sp', [(source, source + steps) for source in range(f...  4.65 us
    ppermute x2, starting transfers between devices, across(): return lax.ppermute(value, 'tp', pairs)  3.9 us
    pallas_call x1, Pallas kernels, qkv(): pl.pallas_call(functools.partial(qkv_kernel, chunks), out_shape=(jax.Shap...  2.97 us
    pallas_call x1, Pallas kernels, attend_near(): pl.pallas_call(near_kernel, out_shape=(jax.ShapeDtypeStruct((CLASSES, 2 *...  1.98 us
  transfers between devices with their start and end apart: 8, of which 3 were waited for; matrix products, arithmetic and copies ran while one was open for 0% of the time, Pallas kernels for 4%

profile of v4, /device:TPU:96, one launch (start us, length us, event | category | flops | bytes accessed | tf_op | source)
XLA Modules:
  0.0 78.5 jit_solution(6262059003193693856)
XLA Ops:
  0.0 0.0 copy-start
  0.0 0.0 copy-start.1
  0.0 3.0 %qkv.1 = (bf16[4,96,128]{2,1,0:T(8,128)(2,1)S(1)}, bf16[4,96,256]{2,1,0:T(8,128)(2,1)S(1)}) custom-call(bf16[384,2048]{1,0:T(8,128)(2,1)} %tok_hbm.1, f32[1,2048]{1,0:T(1,128)} %bitcast.5, bf16[2048,128]{1,0:T(8,128)(2,1)} %wq_hbm.1, bf16[2048,128]{1,0:T(8,128)(2,1)} %wk_hbm.1, bf16[2048,128]{1,0:T(8,128)(2,1)} %wv_hbm.1), custom_call_target="tpu_custom_call" | custom-call | tf_op jit(solution)/shard_map/qkv/pallas_call | solution.py:82
  3.0 6.9 %collective-permute-start = (bf16[4,96,256]{2,1,0:T(8,128)(2,1)S(1)}, bf16[4,96,256]{2,1,0:T(8,128)(2,1)S(1)}, u32[]{:S(2)}, u32[]{:S(2)}) collective-permute-start(bf16[4,96,256]{2,1,0:T(8,128)(2,1)S(1)} %get-tuple-element.13.own), channel_id=1, source_target_pairs={{0,16},{8,24},{16,32},{24,40},{32,48},{40,56},{48,64},{56,72},{64,... | collective-permute-start | bytes 589832 | tf_op jit(solution)/shard_map/ppermute | solution.py:328
  9.9 0.0 copy-done
  9.9 2.0 %collective-permute-start.7 = (bf16[128,2048]{1,0:T(8,128)(2,1)S(1)}, bf16[128,2048]{1,0:T(8,128)(2,1)S(1)}, u32[]{:S(2)}, u32[]{:S(2)}) collective-permute-start(bf16[128,2048]{1,0:T(8,128)(2,1)S(1)} %copy-done), channel_id=1, source_target_pairs={{0,1},{1,0},{2,3},{3,2},{4,5},{5,4},{6,7},{7,6},{8,9},{9,8},{10,11... | collective-permute-start | bytes 1572872 | tf_op jit(solution)/shard_map/ppermute | solution.py:332
  11.9 3.5 %collective-permute-done.rest_1_ = bf16[4,96,256]{2,1,0:T(8,128)(2,1)S(1)} collective-permute-done((bf16[4,96,256]{2,1,0:T(8,128)(2,1)S(1)}, bf16[4,96,256]{2,1,0:T(8,128)(2,1)S(1)}, u32[]{:S(2)}, u32[]{:S(2)}) %collective-permute-start) | collective-permute-done | bytes 196640 | tf_op jit(solution)/shard_map/ppermute | solution.py:328
  15.4 0.7 collective-permute-start.1
  16.1 35.8 %collective-permute-start.4 = (bf16[4,96,256]{2,1,0:T(8,128)(2,1)S(1)}, bf16[4,96,256]{2,1,0:T(8,128)(2,1)S(1)}, u32[]{:S(2)}, u32[]{:S(2)}) collective-permute-start(bf16[4,96,256]{2,1,0:T(8,128)(2,1)S(1)} %get-tuple-element.13.own), channel_id=1, source_target_pairs={{0,8},{8,16},{16,24},{24,32},{32,40},{40,48},{48,56},{56,64},{64,7... | collective-permute-start | bytes 589832 | tf_op jit(solution)/shard_map/ppermute | solution.py:328
  51.9 0.7 collective-permute-start.5
  52.6 0.0 collective-permute-done.1.rest_3_
  52.6 0.7 collective-permute-start.2
  53.3 0.7 collective-permute-start.3
  54.0 1.1 %collective-permute-done.4.rest_0_ = bf16[4,96,256]{2,1,0:T(8,128)(2,1)S(1)} collective-permute-done((bf16[4,96,256]{2,1,0:T(8,128)(2,1)S(1)}, bf16[4,96,256]{2,1,0:T(8,128)(2,1)S(1)}, u32[]{:S(2)}, u32[]{:S(2)}) %collective-permute-start.4) | collective-permute-done | bytes 196640 | tf_op jit(solution)/shard_map/ppermute | solution.py:328
  55.1 0.0 collective-permute-done.5.rest_2_
  55.1 2.0 %attend_near.1 = (f32[4,192,1]{2,1,0:T(8,128)S(1)}, f32[4,192,1]{2,1,0:T(8,128)S(1)}, f32[4,192,128]{2,1,0:T(8,128)S(1)}) custom-call(s32[1]{0:T(128)} %bitcast.sp_ref, bf16[4,96,128]{2,1,0:T(8,128)(2,1)S(1)} %get-tuple-element.12.q_ref, bf16[4,96,256]{2,1,0:T(8,128)(2,1)S(1)} %get-tuple-element.13.own, ...), custom_call_target="tpu_custom_call" | custom-call | tf_op jit(solution)/shard_map/attend_near/pallas_call | solution.py:198
  57.0 0.0 collective-permute-done.3.six
  57.1 0.0 collective-permute-done.2.five
  57.1 0.0 copy-done.1
  57.1 1.3 %attend_far.1 = (bf16[4,48,256]{2,1,0:T(8,128)(2,1)S(1)}, bf16[4,48,256]{2,1,0:T(8,128)(2,1)S(1)}) custom-call(s32[1]{0:T(128)} %bitcast.sp_ref, s32[1]{0:T(128)S(6)} %rem.18.core_ref, bf16[4,96,128]{2,1,0:T(8,128)(2,1)S(1)} %get-tuple-element.12.q_ref, bf16[4,96,256]{2,1,0:T(8,128)(2,1)S(1)} %collective-permute-done.2.five, ...), custom_call_target="tpu_custom_call" | custom-call | tf_op jit(solution)/shard_map/attend_far/pallas_call | solution.py:247
  58.4 2.0 %collective-permute-start.6 = (bf16[4,48,256]{2,1,0:T(8,128)(2,1)S(1)}, bf16[4,48,256]{2,1,0:T(8,128)(2,1)S(1)}, u32[]{:S(2)}, u32[]{:S(2)}) collective-permute-start(bf16[4,48,256]{2,1,0:T(8,128)(2,1)S(1)} %get-tuple-element.18), channel_id=1, source_target_pairs={{0,1},{1,0},{2,3},{3,2},{4,5},{5,4},{6,7},{7,6},{8,9},{9,8},{10,11... | collective-permute-start | bytes 294920 | tf_op jit(solution)/shard_map/ppermute | solution.py:332
  60.3 0.0 collective-permute-done.7.partner
  60.4 1.3 %collective-permute-done.6.got_ref = bf16[4,48,256]{2,1,0:T(8,128)(2,1)S(1)} collective-permute-done((bf16[4,48,256]{2,1,0:T(8,128)(2,1)S(1)}, bf16[4,48,256]{2,1,0:T(8,128)(2,1)S(1)}, u32[]{:S(2)}, u32[]{:S(2)}) %collective-permute-start.6) | collective-permute-done | bytes 98336 | tf_op jit(solution)/shard_map/ppermute | solution.py:332
  61.6 0.5 product.1
  62.2 15.5 %all_to_all.5.parts_ref = bf16[4,784,128]{2,1,0:T(8,128)(2,1)S(1)} all-to-all(bf16[4,784,128]{2,1,0:T(8,128)(2,1)S(1)} %product.1), channel_id=1, replica_groups={{0,2,4,6},{1,3,5,7},{8,10,12,14},{9,11,13,15},{16,18,20,22},{17,19,21,2..., dimensions={0} | all-to-all | bytes 1605632 | tf_op jit(solution)/shard_map/all_to_all | solution.py:357
  77.6 0.8 %finish.1 = bf16[48,2048]{1,0:T(8,128)(2,1)} custom-call(bf16[4,784,128]{2,1,0:T(8,128)(2,1)S(1)} %all_to_all.5.parts_ref), custom_call_target="tpu_custom_call" | custom-call | tf_op jit(solution)/shard_map/finish/pallas_call | solution.py:316
  (1 shorter events, 0.0 us)
Async XLA Ops:
  0.0 9.9 %copy-start = (bf16[128,2048]{1,0:T(8,128)(2,1)S(1)}, bf16[128,2048]{1,0:T(8,128)(2,1)}, u32[]{:S(2)}) copy-start(bf16[128,2048]{1,0:T(8,128)(2,1)} %mine.1) | copy-start | bytes 1572868
  0.0 57.1 %copy-start.1 = (f32[128]{0:T(128)S(1)}, f32[128]{0:T(128)}, u32[]{:S(2)}) copy-start(f32[128]{0:T(128)} %param.12) | copy-start | bytes 1540
  3.0 12.5 %collective-permute-start = (bf16[4,96,256]{2,1,0:T(8,128)(2,1)S(1)}, bf16[4,96,256]{2,1,0:T(8,128)(2,1)S(1)}, u32[]{:S(2)}, u32[]{:S(2)}) collective-permute-start(bf16[4,96,256]{2,1,0:T(8,128)(2,1)S(1)} %get-tuple-element.13.own), channel_id=1, source_target_pairs={{0,16},{8,24},{16,32},{24,40},{32,48},{40,56},{48,64},{56,72},{64,... | collective-permute-start | bytes 589832 | tf_op jit(solution)/shard_map/ppermute | solution.py:328
  9.9 50.4 %collective-permute-start.7 = (bf16[128,2048]{1,0:T(8,128)(2,1)S(1)}, bf16[128,2048]{1,0:T(8,128)(2,1)S(1)}, u32[]{:S(2)}, u32[]{:S(2)}) collective-permute-start(bf16[128,2048]{1,0:T(8,128)(2,1)S(1)} %copy-done), channel_id=1, source_target_pairs={{0,1},{1,0},{2,3},{3,2},{4,5},{5,4},{6,7},{7,6},{8,9},{9,8},{10,11... | collective-permute-start | bytes 1572872 | tf_op jit(solution)/shard_map/ppermute | solution.py:332
  15.4 37.1 %collective-permute-start.1 = (bf16[4,96,256]{2,1,0:T(8,128)(2,1)S(1)}, bf16[4,96,256]{2,1,0:T(8,128)(2,1)S(1)}, u32[]{:S(2)}, u32[]{:S(2)}) collective-permute-start(bf16[4,96,256]{2,1,0:T(8,128)(2,1)S(1)} %collective-permute-done.rest_1_), channel_id=1, source_target_pairs={{16,32},{24,40},{32,48},{40,56},{48,64},{56,72},{64,80},{72,88},{8... | collective-permute-start | bytes 589832 | tf_op jit(solution)/shard_map/ppermute | solution.py:328
  16.1 39.0 %collective-permute-start.4 = (bf16[4,96,256]{2,1,0:T(8,128)(2,1)S(1)}, bf16[4,96,256]{2,1,0:T(8,128)(2,1)S(1)}, u32[]{:S(2)}, u32[]{:S(2)}) collective-permute-start(bf16[4,96,256]{2,1,0:T(8,128)(2,1)S(1)} %get-tuple-element.13.own), channel_id=1, source_target_pairs={{0,8},{8,16},{16,24},{24,32},{32,40},{40,48},{48,56},{56,64},{64,7... | collective-permute-start | bytes 589832 | tf_op jit(solution)/shard_map/ppermute | solution.py:328
  51.9 3.2 %collective-permute-start.5 = (bf16[4,96,256]{2,1,0:T(8,128)(2,1)S(1)}, bf16[4,96,256]{2,1,0:T(8,128)(2,1)S(1)}, u32[]{:S(2)}, u32[]{:S(2)}) collective-permute-start(bf16[4,96,256]{2,1,0:T(8,128)(2,1)S(1)} %collective-permute-done.rest_1_), channel_id=1, source_target_pairs={{16,24},{24,32},{32,40},{40,48},{48,56},{56,64},{64,72},{72,80},{8... | collective-permute-start | bytes 589832 | tf_op jit(solution)/shard_map/ppermute | solution.py:328
  52.6 4.5 %collective-permute-start.2 = (bf16[4,96,256]{2,1,0:T(8,128)(2,1)S(1)}, bf16[4,96,256]{2,1,0:T(8,128)(2,1)S(1)}, u32[]{:S(2)}, u32[]{:S(2)}) collective-permute-start(bf16[4,96,256]{2,1,0:T(8,128)(2,1)S(1)} %collective-permute-done.1.rest_3_), channel_id=1, source_target_pairs={{32,40},{40,48},{48,56},{56,64},{64,72},{72,80},{80,88},{88,96},{9... | collective-permute-start | bytes 589832 | tf_op jit(solution)/shard_map/ppermute | solution.py:328
  53.3 3.8 %collective-permute-start.3 = (bf16[4,32,256]{2,1,0:T(8,128)(2,1)S(1)}, bf16[4,32,256]{2,1,0:T(8,128)(2,1)S(1)}, u32[]{:S(2)}, u32[]{:S(2)}) collective-permute-start(bf16[4,32,256]{2,1,0:T(8,128)(2,1)S(1)} %slice.4), channel_id=1, source_target_pairs={{32,48},{40,56},{48,64},{56,72},{64,80},{72,88},{80,96},{88,104},{... | collective-permute-start | bytes 196616 | tf_op jit(solution)/shard_map/ppermute | solution.py:328
  58.4 3.2 %collective-permute-start.6 = (bf16[4,48,256]{2,1,0:T(8,128)(2,1)S(1)}, bf16[4,48,256]{2,1,0:T(8,128)(2,1)S(1)}, u32[]{:S(2)}, u32[]{:S(2)}) collective-permute-start(bf16[4,48,256]{2,1,0:T(8,128)(2,1)S(1)} %get-tuple-element.18), channel_id=1, source_target_pairs={{0,1},{1,0},{2,3},{3,2},{4,5},{5,4},{6,7},{7,6},{8,9},{9,8},{10,11... | collective-permute-start | bytes 294920 | tf_op jit(solution)/shard_map/ppermute | solution.py:332

commit v5 on v4

--- a/solution.py
+++ b/solution.py
@@ -211,9 +211,11 @@
     )(sp, query, own, *older)
 
 
-def far_kernel(sp_ref, core_ref, q_ref, five, six, top_ref, norm_ref, sum_ref, gain_ref, keep_ref, give_ref, natural):
+def far_kernel(sp_ref, core_ref, q_ref, *rest):
+    blocks = rest[:-7]
+    top_ref, norm_ref, sum_ref, gain_ref, keep_ref, give_ref, natural = rest[-7:]
     share, width = q_ref.shape[1:]
-    count = five.shape[1] + six.shape[1]
+    count = sum(block.shape[1] for block in blocks)
     far = WINDOW_THIRD // CLASSES
     row = lax.broadcasted_iota(jnp.int32, (share, count), 0)
     col = lax.broadcasted_iota(jnp.int32, (share, count), 1)
@@ -222,8 +224,8 @@
     lane = lax.broadcasted_iota(jnp.int32, (share, width), 1)
     for c in range(CLASSES):
         stacked = both_heads(q_ref[c], lane)
-        keys = jnp.concatenate([six[c, :, 0:width], five[c, :, 0:width]], axis=0)
-        values = jnp.concatenate([six[c, :, width : 2 * width], five[c, :, width : 2 * width]], axis=0)
+        keys = jnp.concatenate([block[c, :, 0:width] for block in blocks[::-1]], axis=0)
+        values = jnp.concatenate([block[c, :, width : 2 * width] for block in blocks[::-1]], axis=0)
         score = lax.dot_general(stacked, keys, CONTRACT, preferred_element_type=F32) + bias
         top = jnp.maximum(top_ref[c], jnp.max(score, axis=-1, keepdims=True))
         shrink = jnp.exp(top_ref[c] - top)
@@ -242,17 +244,17 @@
             target[place, :, width : 2 * width] = split(jnp.sum(block * block, axis=-1, keepdims=True), width)
 
 
-def attend_far(sp, core, query, five, six, state, gain, parts):
+def attend_far(sp, core, query, blocks, state, gain, parts):
     share, width = query.shape[1:]
     return pl.pallas_call(
         far_kernel,
         out_shape=(jax.ShapeDtypeStruct((parts, CLASSES * share // (2 * parts), 2 * width), BF16),) * 2,
-        in_specs=[pl.BlockSpec(memory_space=pltpu.SMEM)] * 2 + [pl.BlockSpec(memory_space=VMEM)] * 7,
+        in_specs=[pl.BlockSpec(memory_space=pltpu.SMEM)] * 2 + [pl.BlockSpec(memory_space=VMEM)] * (5 + len(blocks)),
         out_specs=(pl.BlockSpec(memory_space=VMEM),) * 2,
         scratch_shapes=[VMEM((CLASSES * share, width), F32)],
         compiler_params=pltpu.CompilerParams(vmem_limit_bytes=20 << 20),
         name="attend_far",
-    )(sp, core, query, five, six, *state, gain)
+    )(sp, core, query, *blocks, *state, gain)
 
 
 def turned(column_or_row, rows, axis):
@@ -350,8 +352,9 @@
     swap = [(n, n ^ 1) for n in range(n_tp)]
     same_core = [list(range(core, n_tp, 2)) for core in range(2)]
     partner = across(w_out, swap)
-    state = attend_near(sp, query, own, (one, two, three, four))
-    keep, give = attend_far(sp, lax.rem(tp, 2), query, five, six, state, out_gain.reshape(1, -1), n_tp // 2)
+    state = attend_near(sp, query, own, (one, two))
+    far = (three, four, five, six)
+    keep, give = attend_far(sp, lax.rem(tp, 2), query, far, state, out_gain.reshape(1, -1), n_tp // 2)
     got = across(give, swap)
     tiles = product(keep, got, w_out, partner)
     arrived = lax.all_to_all(tiles, "tp", split_axis=0, concat_axis=0, axis_index_groups=same_core, tiled=True)

time: 78.8 us -> 79.3 us (level)
  transfers between devices with their start and end apart: 8 -> 8, of which waited for: 3 -> 3; matrix products, arithmetic and copies ran while one was open for 0% -> 0% of each run, Pallas kernels for 4% -> 5%
where the time goes in v5:
time: 79.3 us; the launch traced here: 78.9 us
  starting transfers between devices  49.3 us (62%)
  blocking collectives  15.5 us (20%)
  Pallas kernels  8.08 us (10%)
  waiting for transfers between devices  5.91 us (7%)
    ppermute x6, starting transfers between devices, ahead(): lax.ppermute(value, 'sp', [(source, source + steps) for source in range(f...  45.4 us
    all_to_all x1, blocking collectives, layer(): lax.all_to_all(tiles, 'tp', split_axis=0, concat_axis=0, axis_index_group...  15.5 us
    ppermute x6, waiting for transfers between devices, ahead(): lax.ppermute(value, 'sp', [(source, source + steps) for source in range(f...  4.65 us
    ppermute x2, starting transfers between devices, across(): return lax.ppermute(value, 'tp', pairs)  3.9 us
    pallas_call x1, Pallas kernels, qkv(): pl.pallas_call(functools.partial(qkv_kernel, chunks), out_shape=(jax.Shap...  2.97 us
    pallas_call x1, Pallas kernels, attend_far(): pl.pallas_call(far_kernel, out_shape=(jax.ShapeDtypeStruct((parts, CLASSE...  1.91 us
    pallas_call x1, Pallas kernels, attend_near(): pl.pallas_call(near_kernel, out_shape=(jax.ShapeDtypeStruct((CLASSES, 2 *...  1.83 us
  transfers between devices with their start and end apart: 8, of which 3 were waited for; matrix products, arithmetic and copies ran while one was open for 0% of the time, Pallas kernels for 5%

profile of v5, /device:TPU:96, one launch (start us, length us, event | category | flops | bytes accessed | tf_op | source)
XLA Modules:
  0.0 78.9 jit_solution(4825472927527430518)
XLA Ops:
  0.0 0.0 copy-start
  0.0 0.0 copy-start.1
  0.0 3.0 %qkv.1 = (bf16[4,96,128]{2,1,0:T(8,128)(2,1)S(1)}, bf16[4,96,256]{2,1,0:T(8,128)(2,1)S(1)}) custom-call(bf16[384,2048]{1,0:T(8,128)(2,1)} %tok_hbm.1, f32[1,2048]{1,0:T(1,128)} %bitcast.5, bf16[2048,128]{1,0:T(8,128)(2,1)} %wq_hbm.1, bf16[2048,128]{1,0:T(8,128)(2,1)} %wk_hbm.1, bf16[2048,128]{1,0:T(8,128)(2,1)} %wv_hbm.1), custom_call_target="tpu_custom_call" | custom-call | tf_op jit(solution)/shard_map/qkv/pallas_call | solution.py:82
  3.0 6.9 %collective-permute-start = (bf16[4,96,256]{2,1,0:T(8,128)(2,1)S(1)}, bf16[4,96,256]{2,1,0:T(8,128)(2,1)S(1)}, u32[]{:S(2)}, u32[]{:S(2)}) collective-permute-start(bf16[4,96,256]{2,1,0:T(8,128)(2,1)S(1)} %get-tuple-element.13.own), channel_id=1, source_target_pairs={{0,16},{8,24},{16,32},{24,40},{32,48},{40,56},{48,64},{56,72},{64,... | collective-permute-start | bytes 589832 | tf_op jit(solution)/shard_map/ppermute | solution.py:330
  9.9 0.0 copy-done
  9.9 2.0 %collective-permute-start.7 = (bf16[128,2048]{1,0:T(8,128)(2,1)S(1)}, bf16[128,2048]{1,0:T(8,128)(2,1)S(1)}, u32[]{:S(2)}, u32[]{:S(2)}) collective-permute-start(bf16[128,2048]{1,0:T(8,128)(2,1)S(1)} %copy-done), channel_id=1, source_target_pairs={{0,1},{1,0},{2,3},{3,2},{4,5},{5,4},{6,7},{7,6},{8,9},{9,8},{10,11... | collective-permute-start | bytes 1572872 | tf_op jit(solution)/shard_map/ppermute | solution.py:334
  11.9 3.5 %collective-permute-done.rest_1_ = bf16[4,96,256]{2,1,0:T(8,128)(2,1)S(1)} collective-permute-done((bf16[4,96,256]{2,1,0:T(8,128)(2,1)S(1)}, bf16[4,96,256]{2,1,0:T(8,128)(2,1)S(1)}, u32[]{:S(2)}, u32[]{:S(2)}) %collective-permute-start) | collective-permute-done | bytes 196640 | tf_op jit(solution)/shard_map/ppermute | solution.py:330
  15.4 0.7 collective-permute-start.2
  16.1 35.8 %collective-permute-start.5 = (bf16[4,96,256]{2,1,0:T(8,128)(2,1)S(1)}, bf16[4,96,256]{2,1,0:T(8,128)(2,1)S(1)}, u32[]{:S(2)}, u32[]{:S(2)}) collective-permute-start(bf16[4,96,256]{2,1,0:T(8,128)(2,1)S(1)} %get-tuple-element.13.own), channel_id=1, source_target_pairs={{0,8},{8,16},{16,24},{24,32},{32,40},{40,48},{48,56},{56,64},{64,7... | collective-permute-start | bytes 589832 | tf_op jit(solution)/shard_map/ppermute | solution.py:330
  51.9 0.7 collective-permute-start.1
  52.6 0.0 collective-permute-done.2.rest_1_
  52.6 0.7 collective-permute-start.3
  53.3 0.7 collective-permute-start.4
  54.0 1.1 %collective-permute-done.5.rest_0_ = bf16[4,96,256]{2,1,0:T(8,128)(2,1)S(1)} collective-permute-done((bf16[4,96,256]{2,1,0:T(8,128)(2,1)S(1)}, bf16[4,96,256]{2,1,0:T(8,128)(2,1)S(1)}, u32[]{:S(2)}, u32[]{:S(2)}) %collective-permute-start.5) | collective-permute-done | bytes 196640 | tf_op jit(solution)/shard_map/ppermute | solution.py:330
  55.1 1.8 %attend_near.1 = (f32[4,192,1]{2,1,0:T(8,128)S(1)}, f32[4,192,1]{2,1,0:T(8,128)S(1)}, f32[4,192,128]{2,1,0:T(8,128)S(1)}) custom-call(s32[1]{0:T(128)} %bitcast.sp_ref, bf16[4,96,128]{2,1,0:T(8,128)(2,1)S(1)} %get-tuple-element.12.q_ref, bf16[4,96,256]{2,1,0:T(8,128)(2,1)S(1)} %get-tuple-element.13.own, ...), custom_call_target="tpu_custom_call" | custom-call | tf_op jit(solution)/shard_map/attend_near/pallas_call | solution.py:198
  56.9 0.0 collective-permute-done.1.rest_0_
  56.9 0.0 collective-permute-done.4.rest_3_
  56.9 0.0 collective-permute-done.3.rest_2_
  56.9 0.0 copy-done.1
  56.9 1.9 %attend_far.1 = (bf16[4,48,256]{2,1,0:T(8,128)(2,1)S(1)}, bf16[4,48,256]{2,1,0:T(8,128)(2,1)S(1)}) custom-call(s32[1]{0:T(128)} %bitcast.sp_ref, s32[1]{0:T(128)S(6)} %rem.18.core_ref, bf16[4,96,128]{2,1,0:T(8,128)(2,1)S(1)} %get-tuple-element.12.q_ref, bf16[4,96,256]{2,1,0:T(8,128)(2,1)S(1)} %collective-permute-done.1.rest_0_, ...), custom_call_target="tpu_custom_call" | custom-call | tf_op jit(solution)/shard_map/attend_far/pallas_call | solution.py:249
  58.9 2.0 %collective-permute-start.6 = (bf16[4,48,256]{2,1,0:T(8,128)(2,1)S(1)}, bf16[4,48,256]{2,1,0:T(8,128)(2,1)S(1)}, u32[]{:S(2)}, u32[]{:S(2)}) collective-permute-start(bf16[4,48,256]{2,1,0:T(8,128)(2,1)S(1)} %get-tuple-element.18), channel_id=1, source_target_pairs={{0,1},{1,0},{2,3},{3,2},{4,5},{5,4},{6,7},{7,6},{8,9},{9,8},{10,11... | collective-permute-start | bytes 294920 | tf_op jit(solution)/shard_map/ppermute | solution.py:334
  60.8 0.0 collective-permute-done.7.partner
  60.8 1.3 %collective-permute-done.6.got_ref = bf16[4,48,256]{2,1,0:T(8,128)(2,1)S(1)} collective-permute-done((bf16[4,48,256]{2,1,0:T(8,128)(2,1)S(1)}, bf16[4,48,256]{2,1,0:T(8,128)(2,1)S(1)}, u32[]{:S(2)}, u32[]{:S(2)}) %collective-permute-start.6) | collective-permute-done | bytes 98336 | tf_op jit(solution)/shard_map/ppermute | solution.py:334
  62.1 0.6 product.1
  62.6 15.5 %all_to_all.5.parts_ref = bf16[4,784,128]{2,1,0:T(8,128)(2,1)S(1)} all-to-all(bf16[4,784,128]{2,1,0:T(8,128)(2,1)S(1)} %product.1), channel_id=1, replica_groups={{0,2,4,6},{1,3,5,7},{8,10,12,14},{9,11,13,15},{16,18,20,22},{17,19,21,2..., dimensions={0} | all-to-all | bytes 1605632 | tf_op jit(solution)/shard_map/all_to_all | solution.py:360
  78.1 0.8 %finish.1 = bf16[48,2048]{1,0:T(8,128)(2,1)} custom-call(bf16[4,784,128]{2,1,0:T(8,128)(2,1)S(1)} %all_to_all.5.parts_ref), custom_call_target="tpu_custom_call" | custom-call | tf_op jit(solution)/shard_map/finish/pallas_call | solution.py:318
  (1 shorter events, 0.0 us)
Async XLA Ops:
  0.0 9.9 %copy-start = (bf16[128,2048]{1,0:T(8,128)(2,1)S(1)}, bf16[128,2048]{1,0:T(8,128)(2,1)}, u32[]{:S(2)}) copy-start(bf16[128,2048]{1,0:T(8,128)(2,1)} %mine.1) | copy-start | bytes 1572868
  0.0 56.9 %copy-start.1 = (f32[128]{0:T(128)S(1)}, f32[128]{0:T(128)}, u32[]{:S(2)}) copy-start(f32[128]{0:T(128)} %param.12) | copy-start | bytes 1540
  3.0 12.5 %collective-permute-start = (bf16[4,96,256]{2,1,0:T(8,128)(2,1)S(1)}, bf16[4,96,256]{2,1,0:T(8,128)(2,1)S(1)}, u32[]{:S(2)}, u32[]{:S(2)}) collective-permute-start(bf16[4,96,256]{2,1,0:T(8,128)(2,1)S(1)} %get-tuple-element.13.own), channel_id=1, source_target_pairs={{0,16},{8,24},{16,32},{24,40},{32,48},{40,56},{48,64},{56,72},{64,... | collective-permute-start | bytes 589832 | tf_op jit(solution)/shard_map/ppermute | solution.py:330
  9.9 50.9 %collective-permute-start.7 = (bf16[128,2048]{1,0:T(8,128)(2,1)S(1)}, bf16[128,2048]{1,0:T(8,128)(2,1)S(1)}, u32[]{:S(2)}, u32[]{:S(2)}) collective-permute-start(bf16[128,2048]{1,0:T(8,128)(2,1)S(1)} %copy-done), channel_id=1, source_target_pairs={{0,1},{1,0},{2,3},{3,2},{4,5},{5,4},{6,7},{7,6},{8,9},{9,8},{10,11... | collective-permute-start | bytes 1572872 | tf_op jit(solution)/shard_map/ppermute | solution.py:334
  15.4 37.1 %collective-permute-start.2 = (bf16[4,96,256]{2,1,0:T(8,128)(2,1)S(1)}, bf16[4,96,256]{2,1,0:T(8,128)(2,1)S(1)}, u32[]{:S(2)}, u32[]{:S(2)}) collective-permute-start(bf16[4,96,256]{2,1,0:T(8,128)(2,1)S(1)} %collective-permute-done.rest_1_), channel_id=1, source_target_pairs={{16,32},{24,40},{32,48},{40,56},{48,64},{56,72},{64,80},{72,88},{8... | collective-permute-start | bytes 589832 | tf_op jit(solution)/shard_map/ppermute | solution.py:330
  16.1 39.0 %collective-permute-start.5 = (bf16[4,96,256]{2,1,0:T(8,128)(2,1)S(1)}, bf16[4,96,256]{2,1,0:T(8,128)(2,1)S(1)}, u32[]{:S(2)}, u32[]{:S(2)}) collective-permute-start(bf16[4,96,256]{2,1,0:T(8,128)(2,1)S(1)} %get-tuple-element.13.own), channel_id=1, source_target_pairs={{0,8},{8,16},{16,24},{24,32},{32,40},{40,48},{48,56},{56,64},{64,7... | collective-permute-start | bytes 589832 | tf_op jit(solution)/shard_map/ppermute | solution.py:330
  51.9 5.0 %collective-permute-start.1 = (bf16[4,96,256]{2,1,0:T(8,128)(2,1)S(1)}, bf16[4,96,256]{2,1,0:T(8,128)(2,1)S(1)}, u32[]{:S(2)}, u32[]{:S(2)}) collective-permute-start(bf16[4,96,256]{2,1,0:T(8,128)(2,1)S(1)} %collective-permute-done.rest_1_), channel_id=1, source_target_pairs={{16,24},{24,32},{32,40},{40,48},{48,56},{56,64},{64,72},{72,80},{8... | collective-permute-start | bytes 589832 | tf_op jit(solution)/shard_map/ppermute | solution.py:330
  52.6 4.3 %collective-permute-start.3 = (bf16[4,96,256]{2,1,0:T(8,128)(2,1)S(1)}, bf16[4,96,256]{2,1,0:T(8,128)(2,1)S(1)}, u32[]{:S(2)}, u32[]{:S(2)}) collective-permute-start(bf16[4,96,256]{2,1,0:T(8,128)(2,1)S(1)} %collective-permute-done.2.rest_1_), channel_id=1, source_target_pairs={{32,40},{40,48},{48,56},{56,64},{64,72},{72,80},{80,88},{88,96},{9... | collective-permute-start | bytes 589832 | tf_op jit(solution)/shard_map/ppermute | solution.py:330
  53.3 3.6 %collective-permute-start.4 = (bf16[4,32,256]{2,1,0:T(8,128)(2,1)S(1)}, bf16[4,32,256]{2,1,0:T(8,128)(2,1)S(1)}, u32[]{:S(2)}, u32[]{:S(2)}) collective-permute-start(bf16[4,32,256]{2,1,0:T(8,128)(2,1)S(1)} %slice.4), channel_id=1, source_target_pairs={{32,48},{40,56},{48,64},{56,72},{64,80},{72,88},{80,96},{88,104},{... | collective-permute-start | bytes 196616 | tf_op jit(solution)/shard_map/ppermute | solution.py:330
  58.9 3.2 %collective-permute-start.6 = (bf16[4,48,256]{2,1,0:T(8,128)(2,1)S(1)}, bf16[4,48,256]{2,1,0:T(8,128)(2,1)S(1)}, u32[]{:S(2)}, u32[]{:S(2)}) collective-permute-start(bf16[4,48,256]{2,1,0:T(8,128)(2,1)S(1)} %get-tuple-element.18), channel_id=1, source_target_pairs={{0,1},{1,0},{2,3},{3,2},{4,5},{5,4},{6,7},{7,6},{8,9},{9,8},{10,11... | collective-permute-start | bytes 294920 | tf_op jit(solution)/shard_map/ppermute | solution.py:334
